TPU v7x, 256 devices: a whole 4x4x8 slice. The times are simulated.
256 devices in a mesh: sp: 16 (over y, x), tp: 16 (over z, core).
Axes of the slice: x: 4, y: 4, z: 8, core: 2. Of those that a mesh axis runs over, the one named last changes fastest.
Arguments:
- mix_in: bfloat16 [16384, 2048], P('sp', 'tp'), may hold values from -8 to 8
- gate_in: bfloat16 [16384, 2048], P('sp', 'tp'), may hold values from -6 to 6
- conv_w: float32 [4, 2048], P(None, 'tp'), may hold values from -3 to 3
- conv_b: float32 [2048], P('tp'), may hold values from -3 to 3
- decay_param: float32 [2, 2048], P(None, 'tp')
- recur_gate: float32 [2, 32, 64, 64], P(None, 'tp'), may hold values from -0.75 to 0.75
- recur_bias: float32 [2, 2048], P(None, 'tp'), may hold values from -4 to 4
- input_gate: float32 [2, 32, 64, 64], P(None, 'tp'), may hold values from -0.75 to 0.75
- input_bias: float32 [2, 2048], P(None, 'tp'), may hold values from -4 to 4
- residual: bfloat16 [16384, 2048], P(('sp', 'tp')), may hold values from -6 to 6
- out_proj: bfloat16 [2048, 2048], replicated, may hold values from -0.125 to 0.125
- norm_gain: float32 [3, 2048], replicated, may hold values from 0.1 to 1.9
- routes: int32 [16384, 2], P('sp'), may hold values from 0 to 15, all different within a row; in each aligned block of 64 rows (0 to 63, 64 to 127, ...) at most 16 rows name the same one
- route_wt: float32 [16384, 2], P('sp'), may hold values from 0.1 to 1
- exp_gate: bfloat16 [16, 2048, 1024], P('sp', None, 'tp'), may hold values from -0.125 to 0.125
- exp_up: bfloat16 [16, 2048, 1024], P('sp', None, 'tp'), may hold values from -0.125 to 0.125
- exp_down: bfloat16 [16, 1024, 2048], P('sp', 'tp'), may hold values from -0.1875 to 0.1875
Outputs:
- final: bfloat16 [16384, 2048], P(('sp', 'tp'))
Inputs may be any that keep to these rules, and one draw needn't show every extreme that they name: `routes`: in each aligned block of 64 tokens (the rows of one device in the expert layer) no expert is named more than 16 times, and in some block some expert exactly 16 times; a token's 2 experts differ.
All inputs are finite; a program needn't handle non-finite values.
Results may differ from a plain program's by a relative error of at most 0.008.
Values may be sent and summed in bfloat16 or wider, within the bound.
A program may use at most 128 MiB of HBM per device.

v0:
```python
import jax
import jax.numpy as jnp
from jax import lax
from jax.sharding import PartitionSpec as P

EPSILON = 1e-06
HIGHEST_MODE = lax.Precision.HIGHEST


def extended(cells, sides, width):
    for axis, dim in sides:
        count = lax.axis_size(axis)
        ends = count - 1
        head = lax.slice_in_dim(cells, 0, width, axis=dim)
        tail = lax.slice_in_dim(cells, cells.shape[dim] - width, cells.shape[dim], axis=dim)
        cells = jnp.concatenate(
            [
                lax.ppermute(tail, axis, [(i, (i + 1) % count) for i in range(ends)]),
                cells,
                lax.ppermute(head, axis, [((i + 1) % count, i) for i in range(ends)]),
            ],
            axis=dim,
        )
    return cells


def copy_for_each(array, axis):
    copies = jnp.broadcast_to(array, (lax.axis_size(axis), *array.shape))
    return lax.all_to_all(copies, axis, split_axis=0, concat_axis=0, tiled=True)


def collected_together(array, axis):
    leaves = jax.tree.leaves(array)
    order = sorted(range(len(leaves)), key=lambda k: -leaves[k].size)
    width = (1, *leaves[order[0]].shape)[-1]
    lines = [
        jnp.pad(leaves[k].reshape(-1), (0, -leaves[k].size % width)).reshape(-1, width)
        for k in order
    ]
    both, at, found = (copy_for_each(jnp.concatenate(lines), axis), 0, {})
    for k, line in zip(order, lines):
        piece = both[:, at : at + len(line)].reshape(len(both), -1)
        found[k] = piece[:, : leaves[k].size].reshape(-1, *leaves[k].shape)
        at += len(line)
    numbers = iter(range(len(leaves)))
    return jax.tree.map(lambda _: found[next(numbers)], array)


def folded_in_pairs(pieces, combine):
    while len(jax.tree.leaves(pieces)[0]) > 1:
        pieces = jax.vmap(combine)(
            *(jax.tree.map(lambda part: part[side::2], pieces) for side in (0, 1))
        )
    return jax.tree.map(lambda part: part[0], pieces)


def carried_in(array, axis, combine, identity, reverse):
    length, here = (lax.axis_size(axis), lax.axis_index(axis))
    passed = jnp.arange(length) > here if reverse else jnp.arange(length) < here

    def kept(part, zero, own):
        part = jnp.where(
            passed.reshape(-1, *(1 for _ in own.shape)), part, jnp.asarray(zero, own.dtype)
        )
        return part[::-1] if reverse else part

    pieces = collected_together(array, axis)
    return folded_in_pairs(jax.tree.map(kept, pieces, identity, array), combine)


def gather_turned(arrays, axis, dims):
    turned = [jnp.moveaxis(a, dim, 0) for a, dim in zip(arrays, dims)]
    widths = [t[0].size for t in turned]
    both = jnp.concatenate([t.reshape(-1, w) for t, w in zip(turned, widths)], axis=1)
    filled = lax.all_gather(both, axis, axis=0, tiled=True)
    tiles = jnp.split(filled, [sum(widths[:k]) for k in range(1, len(widths))], axis=1)
    return tuple(
        (
            jnp.moveaxis(b.reshape(-1, *t.shape[1:]), 0, dim)
            for b, t, dim in zip(tiles, turned, dims)
        )
    )


def norm_rows(values, gain):
    floats = values.astype(jnp.float32)
    return floats * lax.rsqrt(jnp.mean(floats * floats, axis=-1, keepdims=True) + EPSILON) * gain


def pair_join(earlier, later_pair):
    return (earlier[0] * later_pair[0], later_pair[0] * earlier[1] + later_pair[1])


def slot_table(route_rows, experts, capacity):
    row_count, top_count = route_rows.shape
    flattened = route_rows.reshape(row_count * top_count)
    matches = (flattened[:, None] == jnp.arange(experts, dtype=jnp.int32)[None, :]).astype(
        jnp.int32
    )
    earlier_hits = jnp.cumsum(matches, axis=0) - matches
    position = jnp.sum(earlier_hits * matches, axis=1)
    return (flattened * capacity + position).reshape(row_count, top_count)


def weight_table(slots, route_weights, total_slots):
    matches = slots[..., None] == jnp.arange(total_slots, dtype=jnp.int32)
    return jnp.sum(jnp.where(matches, route_weights[..., None], 0.0), axis=-2)


def block_matrix(blocks):
    heads, head_dim, _ = blocks.shape
    identity = jnp.eye(heads, dtype=blocks.dtype)
    return jnp.einsum("hij,hg->higj", blocks, identity).reshape(heads * head_dim, heads * head_dim)


def coefficients(conv_out, recur_blocks, recur_bias, input_blocks, input_bias, decay_param):
    recur_pre = jnp.dot(conv_out, block_matrix(recur_blocks), precision=HIGHEST_MODE)
    input_pre = jnp.dot(conv_out, block_matrix(input_blocks), precision=HIGHEST_MODE)
    recur_act = jax.nn.sigmoid(recur_pre + recur_bias)
    input_act = jax.nn.sigmoid(input_pre + input_bias)
    log_decay = -8.0 * recur_act * jax.nn.softplus(-decay_param)
    return (jnp.exp(log_decay), jnp.sqrt(-jnp.expm1(2.0 * log_decay)) * (input_act * conv_out))


def on_device(
    mix_in,
    gate_in,
    conv_w,
    conv_b,
    decay_param,
    recur_gate,
    recur_bias,
    input_gate,
    input_bias,
    residual,
    out_proj,
    norm_gain,
    routes,
    route_wt,
    exp_gate,
    exp_up,
    exp_down,
):
    seq_len = mix_in.shape[0]
    padded = extended(mix_in, (("sp", 0),), 2).astype(jnp.float32)
    conv_out = conv_b + padded[0:seq_len] * conv_w[0]
    for tap in range(1, conv_w.shape[0]):
        conv_out = conv_out + padded[tap : tap + seq_len] * conv_w[tap]
    fwd_decay, fwd_drive = coefficients(
        conv_out, recur_gate[0], recur_bias[0], input_gate[0], input_bias[0], decay_param[0]
    )
    bwd_decay, bwd_drive = coefficients(
        conv_out, recur_gate[1], recur_bias[1], input_gate[1], input_bias[1], decay_param[1]
    )
    fwd_prod, fwd_state = lax.associative_scan(pair_join, (fwd_decay, fwd_drive), axis=0)
    bwd_prod, bwd_state = lax.associative_scan(
        pair_join, (jnp.flip(bwd_decay, 0), jnp.flip(bwd_drive, 0)), axis=0
    )
    identity = (jnp.ones_like(fwd_prod[-1]), jnp.zeros_like(fwd_state[-1]))
    fwd_enter = carried_in((fwd_prod[-1], fwd_state[-1]), "sp", pair_join, identity, False)[1]
    bwd_enter = carried_in((bwd_prod[-1], bwd_state[-1]), "sp", pair_join, identity, True)[1]
    state_sum = fwd_state + fwd_prod * fwd_enter + jnp.flip(bwd_state + bwd_prod * bwd_enter, 0)
    mixed = (state_sum * jax.nn.gelu(gate_in.astype(jnp.float32))).astype(jnp.bfloat16)
    tok_rows = lax.all_to_all(mixed, "tp", split_axis=0, concat_axis=1, tiled=True)
    proj = jnp.dot(tok_rows, out_proj, preferred_element_type=jnp.float32).astype(jnp.bfloat16)
    proj = lax.optimization_barrier(proj)
    stream = (residual.astype(jnp.float32) + norm_rows(proj, norm_gain[0])).astype(jnp.bfloat16)
    stream = lax.optimization_barrier(stream)
    normed = norm_rows(stream, norm_gain[1]).astype(jnp.bfloat16)
    sp_count = lax.axis_size("sp")
    row_count = residual.shape[0]
    width_model = residual.shape[1]
    top_count = routes.shape[1]
    local_experts = exp_gate.shape[0]
    experts = local_experts * sp_count
    capacity = 2 * row_count * top_count // experts
    total_slots = experts * capacity
    own_start = lax.axis_index("tp") * row_count
    own_routes = lax.dynamic_slice_in_dim(routes, own_start, row_count, 0)
    own_weights = lax.dynamic_slice_in_dim(route_wt, own_start, row_count, 0)
    own_slots = slot_table(own_routes, experts, capacity)
    selector = jnp.sum(
        (own_slots[:, :, None] == jnp.arange(total_slots, dtype=jnp.int32)).astype(jnp.bfloat16),
        axis=1,
    )
    outgoing = jnp.einsum("rs,rd->sd", selector, normed, preferred_element_type=jnp.float32).astype(
        jnp.bfloat16
    )
    arrived = lax.all_to_all(
        outgoing.reshape(experts, capacity, width_model),
        "sp",
        split_axis=0,
        concat_axis=1,
        tiled=True,
    )
    gate_full, up_full = gather_turned((exp_gate, exp_up), "tp", (2, 2))
    gate_act = jnp.einsum("emd,edf->emf", arrived, gate_full, preferred_element_type=jnp.float32)
    up_act = jnp.einsum("emd,edf->emf", arrived, up_full, preferred_element_type=jnp.float32)
    hidden = (jax.nn.silu(gate_act) * up_act).astype(jnp.bfloat16)
    summed = jnp.einsum(
        "emf,efd->emd",
        hidden,
        lax.all_gather(exp_down, "tp", axis=1, tiled=True),
        preferred_element_type=jnp.float32,
    )
    out_rows = summed.astype(jnp.bfloat16).reshape(local_experts, sp_count, capacity, width_model)
    returned = lax.all_to_all(out_rows, "sp", split_axis=1, concat_axis=0, tiled=True)
    values = returned.reshape(total_slots, width_model).astype(jnp.float32)
    own_table = weight_table(own_slots, own_weights, total_slots)
    mixture = jnp.dot(own_table, values, precision=HIGHEST_MODE).astype(jnp.bfloat16)
    mixture = lax.optimization_barrier(mixture)
    return (stream.astype(jnp.float32) + norm_rows(mixture, norm_gain[2])).astype(jnp.bfloat16)


def solution(mesh):
    return jax.shard_map(
        on_device,
        mesh=mesh,
        in_specs=(
            P("sp", "tp"),
            P("sp", "tp"),
            P(None, "tp"),
            P("tp"),
            P(None, "tp"),
            P(None, "tp", None, None),
            P(None, "tp"),
            P(None, "tp", None, None),
            P(None, "tp"),
            P(("sp", "tp"), None),
            P(),
            P(),
            P("sp", None),
            P("sp", None),
            P("sp", None, "tp"),
            P("sp", None, "tp"),
            P("sp", "tp", None),
        ),
        out_specs=P(("sp", "tp"), None),
        check_vma=False,
    )
```

profile of v0, /device:TPU:1, one launch (start us, length us, event | category | flops | bytes accessed | tf_op | source)
XLA Modules:
  0.0 247.0 jit_solution(15840716906587601891)
XLA Ops:
  6.5 1.9 pad_maximum_fusion
  9.2 3.9 %collective-permute-start = (bf16[2,128]{1,0:T(2,128)(2,1)S(1)}, bf16[2,128]{1,0:T(2,128)(2,1)S(1)}, u32[]{:S(2)}, u32[]{:S(2)}) collective-permute-start(bf16[2,128]{1,0:T(2,128)(2,1)S(1)} %get-tuple-element.14), channel_id=1, source_target_pairs={{0,16},{16,32},{32,48},{48,64},{64,80},{80,96},{96,112},{112,128},... | collective-permute-start | bytes 1544 | tf_op jit(solution)/shard_map/ppermute | solution.py:18
  20.7 2.0 concatenate.120
  49.8 1.7 fusion.91
  51.5 2.1 fusion.14
  97.8 7.7 %all-to-all-start = ((f32[16,2,128]{2,1,0:T(2,128)}), f32[16,2,128]{2,1,0:T(2,128)}, u32[]{:S(2)}, u32[]{:S(2)}) async-start(f32[16,2,128]{2,1,0:T(2,128)} %broadcast_in_dim.59), calls=%async_computation | async-start | bytes 32768 | tf_op jit(solution)/shard_map/all_to_all | solution.py:29
  123.1 3.0 %slice.1014 = f32[511,128]{1,0:T(8,128)} reverse(f32[511,128]{1,0:T(8,128)} %slice.1013), dimensions={0} | reverse | bytes 523264 | tf_op jit(solution)/shard_map/slice | solution.py:156
  126.1 1.4 slice.936
  130.1 1.4 pad_maximum_fusion.3
  132.6 1.6 pad.303
  134.3 2.7 %pad.302 = f32[1024,128]{1,0:T(8,128)} pad(f32[512,128]{1,0:T(8,128)} %pad_maximum_fusion.3, f32[]{:T(128)} %constant.17.clone.1), padding=0_1_1x0_0_0 | pad | bytes 786436 | tf_op jit(solution)/shard_map/pad | solution.py:156
  138.3 6.6 %all-to-all-start.1 = ((f32[16,2,128]{2,1,0:T(2,128)}), f32[16,2,128]{2,1,0:T(2,128)S(1)}, u32[]{:S(2)}, u32[]{:S(2)}) async-start(f32[16,2,128]{2,1,0:T(2,128)} %broadcast_in_dim.63), calls=%async_computation.1 | async-start | bytes 32768 | tf_op jit(solution)/shard_map/all_to_all | solution.py:29
  146.7 4.6 %all-to-all-done.1 = f32[16,2,128]{2,1,0:T(2,128)S(1)} async-done(((f32[16,2,128]{2,1,0:T(2,128)}), f32[16,2,128]{2,1,0:T(2,128)S(1)}, u32[]{:S(2)}, u32[]{:S(2)}) %all-to-all-start.1) | async-done | bytes 16416 | tf_op jit(solution)/shard_map/all_to_all | solution.py:29
  151.7 2.2 multiply_add_fusion
  153.9 3.4 %rev.8 = f32[1024,128]{1,0:T(8,128)S(1)} reverse(f32[1024,128]{1,0:T(8,128)} %multiply_add_fusion), dimensions={0} | reverse | bytes 1048576 | tf_op jit(solution)/shard_map/jit(_flip)/rev | solution.py:162
  157.4 2.0 fusion.47
  159.3 11.7 %all-to-all-start.2 = ((bf16[16,64,128]{2,1,0:T(8,128)(2,1)}), bf16[16,64,128]{2,1,0:T(8,128)(2,1)S(1)}, u32[]{:S(2)}, u32[]{:S(2)}) async-start(bf16[16,64,128]{2,1,0:T(8,128)(2,1)} %bitcast.24), calls=%async_computation.2 | async-start | bytes 524288 | tf_op jit(solution)/shard_map/all_to_all | solution.py:164
  171.2 11.4 %all-to-all-done.2 = bf16[16,64,128]{2,1,0:T(8,128)(2,1)S(1)} async-done(((bf16[16,64,128]{2,1,0:T(8,128)(2,1)}), bf16[16,64,128]{2,1,0:T(8,128)(2,1)S(1)}, u32[]{:S(2)}, u32[]{:S(2)}) %all-to-all-start.2) | async-done | bytes 262176 | tf_op jit(solution)/shard_map/all_to_all | solution.py:164
  182.6 5.0 %convolution_convert_fusion.2 = bf16[64,2048]{1,0:T(8,128)(2,1)S(1)} fusion(bf16[2048,2048]{1,0:T(8,128)(2,1)} %param.27, bf16[16,64,128]{2,1,0:T(8,128)(2,1)S(1)} %all-to-all-done.2), kind=kOutput, calls=%fused_computation.9 | convolution fusion | flops 537001984 | bytes 8912896 | tf_op jit(solution)/shard_map/dot_general | solution.py:165
  188.6 19.8 %all_to_all.47 = bf16[16,16,2048]{2,1,0:T(8,128)(2,1)S(1)} all-to-all(bf16[16,16,2048]{2,1,0:T(8,128)(2,1)S(1)} %bitcast.114), channel_id=1, replica_groups=mesh['sp'=16,'tp'=16] {'sp'}, dimensions={0} | all-to-all | bytes 2097152 | tf_op jit(solution)/shard_map/all_to_all | solution.py:189
  208.4 3.5 %fusion.1 = f32[256,1024]{1,0:T(8,128)S(1)} fusion(bf16[256,2048]{1,0:T(8,128)(2,1)S(1)} %bitcast.115, bf16[1024,4096]{1,0:T(8,128)(2,1)} %all-gather.3.cloned.1.call-done), kind=kOutput, calls=%fused_computation.3 | convolution fusion | flops 1073741824 | bytes 6291456 | tf_op jit(solution)/shard_map/emd,edf->emf/dot_general | solution.py:197
  212.0 6.9 %fusion.4 = bf16[256,2048]{1,0:T(8,128)(2,1)} fusion(bf16[1,1024,2048]{2,1,0:T(8,128)(2,1)} %all-gather.5.cloned.1.call-done, bf16[256,2048]{1,0:T(8,128)(2,1)S(1)} %bitcast.116, bf16[1024,4096]{1,0:T(8,128)(2,1)} %all-gather.3.cloned.1.call-done, f32[256,1024]{1,0:T(8,128)S(1)} %fusion.1), kind=kOutput, calls=%fused_computation.6 | convolution fusion | flops 2149580800 | bytes 11534336 | tf_op jit(solution)/shard_map/emf,efd->emd/dot_general | solution.py:200
  218.9 3.7 %all-to-all-start.4 = ((bf16[1,16,16,2048]{3,2,0,1:T(8,128)(2,1)}), bf16[1,16,16,2048]{3,2,0,1:T(8,128)(2,1)S(1)}, u32[]{:S(2)}, u32[]{:S(2)}) async-start(bf16[1,16,16,2048]{3,2,0,1:T(8,128)(2,1)} %bitcast.42), calls=%async_computation.4 | async-start | bytes 2097152 | tf_op jit(solution)/shard_map/all_to_all | solution.py:207
  223.4 15.0 %all-to-all-done.4 = bf16[1,16,16,2048]{3,2,0,1:T(8,128)(2,1)S(1)} async-done(((bf16[1,16,16,2048]{3,2,0,1:T(8,128)(2,1)}), bf16[1,16,16,2048]{3,2,0,1:T(8,128)(2,1)S(1)}, u32[]{:S(2)}, u32[]{:S(2)}) %all-to-all-start.4) | async-done | bytes 1048608 | tf_op jit(solution)/shard_map/all_to_all | solution.py:207
  (435 shorter events, 106.9 us)
Async XLA Ops:
  6.5 9.5 %copy-start = (s32[1024,2]{0,1:T(2,128)S(1)}, s32[1024,2]{0,1:T(2,128)}, u32[]{:S(2)}) copy-start(s32[1024,2]{0,1:T(2,128)} %param.29) | copy-start | bytes 24580
  6.5 201.9 %all-gather.3.cloned.1.call-start = ((), (), s32[]{:S(2)}) async-start(), calls=%async_computation.5 | async-start | bytes 8912896 | tf_op jit(solution)/shard_map/all_gather | solution.py:75
  8.4 203.5 %all-gather.5.cloned.1.call-start = ((), (), s32[]{:S(2)}) async-start(), calls=%async_computation.6 | async-start | bytes 4456448 | tf_op jit(solution)/shard_map/all_gather | solution.py:203
  9.2 11.6 %collective-permute-start = (bf16[2,128]{1,0:T(2,128)(2,1)S(1)}, bf16[2,128]{1,0:T(2,128)(2,1)S(1)}, u32[]{:S(2)}, u32[]{:S(2)}) collective-permute-start(bf16[2,128]{1,0:T(2,128)(2,1)S(1)} %get-tuple-element.14), channel_id=1, source_target_pairs={{0,16},{16,32},{32,48},{48,64},{64,80},{80,96},{96,112},{112,128},... | collective-permute-start | bytes 1544 | tf_op jit(solution)/shard_map/ppermute | solution.py:18
  13.1 7.6 %collective-permute-start.1 = (bf16[2,128]{1,0:T(2,128)(2,1)S(1)}, bf16[2,128]{1,0:T(2,128)(2,1)S(1)}, u32[]{:S(2)}, u32[]{:S(2)}) collective-permute-start(bf16[2,128]{1,0:T(2,128)(2,1)S(1)} %get-tuple-element.13), channel_id=1, source_target_pairs={{16,0},{32,16},{48,32},{64,48},{80,64},{96,80},{112,96},{128,112},... | collective-permute-start | bytes 1544 | tf_op jit(solution)/shard_map/ppermute | solution.py:20
  23.7 0.8 copy-start.3
  25.4 29.9 %copy-start.1 = (f32[1024,128]{1,0:T(8,128)}, f32[1024,128]{1,0:T(8,128)S(1)}, u32[]{:S(2)}) copy-start(f32[1024,128]{1,0:T(8,128)S(1)} %fusion.25) | copy-start | bytes 1572868
  55.8 40.9 %copy-start.2 = (f32[511,128]{1,0:T(8,128)S(1)}, f32[511,128]{1,0:T(8,128)}, u32[]{:S(2)}) copy-start(f32[511,128]{1,0:T(8,128)} %slice.817) | copy-start | bytes 784900
  56.2 40.6 %copy-start.8 = (f32[1,128]{1,0:T(1,128)S(1)}, f32[1,128]{1,0:T(1,128)}, u32[]{:S(2)}) copy-start(f32[1,128]{1,0:T(1,128)} %slice.1083) | copy-start | bytes 1540
  56.6 40.5 %slice-start = ((f32[1024,128]{1,0:T(8,128)}), f32[1,128]{1,0:T(1,128)S(1)}, s32[]{:S(2)}) async-start(f32[1024,128]{1,0:T(8,128)} %copy-done.1), calls=%async_computation.7 | async-start | bytes 1024 | tf_op jit(solution)/shard_map/slice | solution.py:155
  97.8 39.9 %all-to-all-start = ((f32[16,2,128]{2,1,0:T(2,128)}), f32[16,2,128]{2,1,0:T(2,128)}, u32[]{:S(2)}, u32[]{:S(2)}) async-start(f32[16,2,128]{2,1,0:T(2,128)} %broadcast_in_dim.59), calls=%async_computation | async-start | bytes 32768 | tf_op jit(solution)/shard_map/all_to_all | solution.py:29
  112.8 38.5 %copy-start.7 = (pred[16]{0:T(512)(128)(4,1)S(1)}, pred[16]{0:T(512)(128)(4,1)}, u32[]{:S(2)}) copy-start(pred[16]{0:T(512)(128)(4,1)} %get-tuple-element.140) | copy-start | bytes 52
  123.1 48.0 %copy-start.6 = (s32[64,2]{0,1:T(2,128)S(1)}, s32[64,2]{0,1:T(2,128)}, u32[]{:S(2)}) copy-start(s32[64,2]{0,1:T(2,128)} %copy.35) | copy-start | bytes 1540
  123.1 48.0 %copy-start.5 = (f32[3,2048]{1,0:T(4,128)S(1)}, f32[3,2048]{1,0:T(4,128)}, u32[]{:S(2)}) copy-start(f32[3,2048]{1,0:T(4,128)} %param.28) | copy-start | bytes 73732
  138.3 13.1 %all-to-all-start.1 = ((f32[16,2,128]{2,1,0:T(2,128)}), f32[16,2,128]{2,1,0:T(2,128)S(1)}, u32[]{:S(2)}, u32[]{:S(2)}) async-start(f32[16,2,128]{2,1,0:T(2,128)} %broadcast_in_dim.63), calls=%async_computation.1 | async-start | bytes 32768 | tf_op jit(solution)/shard_map/all_to_all | solution.py:29
  159.3 23.3 %all-to-all-start.2 = ((bf16[16,64,128]{2,1,0:T(8,128)(2,1)}), bf16[16,64,128]{2,1,0:T(8,128)(2,1)S(1)}, u32[]{:S(2)}, u32[]{:S(2)}) async-start(bf16[16,64,128]{2,1,0:T(8,128)(2,1)} %bitcast.24), calls=%async_computation.2 | async-start | bytes 524288 | tf_op jit(solution)/shard_map/all_to_all | solution.py:164
  171.2 16.6 %copy-start.4 = (bf16[64,2048]{1,0:T(8,128)(2,1)S(1)}, bf16[64,2048]{1,0:T(8,128)(2,1)}, u32[]{:S(2)}) copy-start(bf16[64,2048]{1,0:T(8,128)(2,1)} %param.26) | copy-start | bytes 786436
  218.9 19.5 %all-to-all-start.4 = ((bf16[1,16,16,2048]{3,2,0,1:T(8,128)(2,1)}), bf16[1,16,16,2048]{3,2,0,1:T(8,128)(2,1)S(1)}, u32[]{:S(2)}, u32[]{:S(2)}) async-start(bf16[1,16,16,2048]{3,2,0,1:T(8,128)(2,1)} %bitcast.42), calls=%async_computation.4 | async-start | bytes 2097152 | tf_op jit(solution)/shard_map/all_to_all | solution.py:207
Sparse Core Ops, SparseCore 0:
  9.2 60.0 all-gather.2
  71.1 40.5 all-gather.4
where the time goes:
time: 249 us; the launch traced here: 247 us
  local copies, waits for them, and re-layouts  71.7 us (29%)
  other arithmetic  52.7 us (21%)
  starting transfers between devices  34.9 us (14%)
  waiting for transfers between devices  31.2 us (13%)
  matrix products  21.8 us (9%)
  blocking collectives  19.8 us (8%)
  between operations  14.9 us (6%)
    slice x74, local copies, waits for them, and re-layouts, on_device(): lax.associative_scan(pair_join, (jnp.flip(bwd_decay, 0), jnp.flip(bwd_dri...  26 us
    slice x69, local copies, waits for them, and re-layouts, on_device(): lax.associative_scan(pair_join, (fwd_decay, fwd_drive), axis=0)  21 us
    all_to_all x1, blocking collectives, on_device(): lax.all_to_all(outgoing.reshape(experts, capacity, width_model), 'sp', sp...  19.8 us
    all_to_all x1, waiting for transfers between devices, on_device(): lax.all_to_all(out_rows, 'sp', split_axis=1, concat_axis=0, tiled=True)  15 us
    all_to_all x2, starting transfers between devices, copy_for_each(): return lax.all_to_all(copies, axis, split_axis=0, concat_axis=0, tiled=True)  14.3 us
    concatenate x18, other arithmetic, on_device(): lax.associative_scan(pair_join, (jnp.flip(bwd_decay, 0), jnp.flip(bwd_dri...  12.9 us
    add x36, other arithmetic, pair_join(): later_pair[0] * earlier[1] + later_pair[1]  12.6 us
    all_to_all x1, starting transfers between devices, on_device(): lax.all_to_all(mixed, 'tp', split_axis=0, concat_axis=1, tiled=True)  11.7 us
  transfers between devices with their start and end apart: 8, of which 3 were waited for; matrix products, arithmetic and copies ran while one was open for 55% of the time, Pallas kernels for 0%

commit v1 on v0

v1 whole, which is shorter than its diff:
```python
import functools

import jax
import jax.numpy as jnp
from jax import lax
from jax.experimental import pallas as pl
from jax.experimental.pallas import tpu as pltpu
from jax.sharding import PartitionSpec as P

EPSILON = 1e-06
HIGHEST_MODE = lax.Precision.HIGHEST
MESH = pl.DeviceIdType.MESH
F32, BF16 = jnp.float32, jnp.bfloat16
SEGMENTS = 8
CHUNKS = 4


def hint(value, step):
    return pl.multiple_of(value, step)


def blocked_all(copy_ref, sem):
    pltpu.make_async_copy(copy_ref, copy_ref, sem).wait()


def root_mean(values):
    return lax.rsqrt(jnp.mean(values * values, axis=-1, keepdims=True) + EPSILON)


def ring_plan(nz):
    far, near = nz // 2, nz - 1 - nz // 2
    plans = []
    for direction in (0, 1):
        hops = lambda piece: far if (piece % 2 == direction) else near
        order = []
        groups = [(0, 1)] + [(2 + 2 * k, 3 + 2 * k) for k in range(CHUNKS // 2)]
        for group in groups:
            first = group if direction == 0 else group[::-1]
            for hop in range(1, far + 1):
                for piece in first:
                    if hop <= hops(piece):
                        order.append((piece, hop))
        plans.append(order)
    return plans


def kernel(
    n_sp,
    n_tp,
    mix_h,
    gate_h,
    conv_w,
    conv_b,
    decay,
    rg,
    rb,
    ig,
    ib,
    resid_h,
    oproj_h,
    gain,
    routes_h,
    wts_h,
    wg_h,
    wu_h,
    wd_h,
    out_ref,
    mixv,
    gatev,
    residv,
    oproj,
    routv,
    wtsv,
    halo,
    xpad,
    conv_s,
    wcat,
    ca0,
    cd0,
    ca1,
    cd1,
    stats,
    mixed,
    tokb,
    pbuf,
    stream_s,
    normed,
    outg,
    arr,
    wg,
    wu,
    wd,
    hid,
    outb,
    ret,
    wtab,
    load_sem,
    halo_send,
    halo_recv,
    stat_sem,
    tok_sem,
    disp_send,
    disp_recv,
    fwd_sem,
    hid_sem,
    pre_sem,
    ring_send,
    ring_recv,
    ret_send,
    ret_recv,
):
    nz = n_tp // 2
    sp, tp = lax.axis_index("sp"), lax.axis_index("tp")
    z, core = tp // 2, lax.rem(tp, 2)
    other = 1 - core
    sibling = 2 * z + other
    seq, chans = mix_h.shape
    rows, width = resid_h.shape
    half = width // 2
    hs = wg_h.shape[0]
    cap = outg.shape[0] // n_sp
    slots = n_sp * cap
    seg = seq // SEGMENTS
    cw = half // CHUNKS

    def load(src, dst, k):
        copy = pltpu.make_async_copy(src, dst, load_sem.at[k])
        copy.start()
        return copy

    own_rows = hint(tp * rows, rows)
    l_mix = load(mix_h, mixv, 0)
    l_gate = load(gate_h, gatev, 1)
    l_wg = load(wg_h, wg.at[z], 2)
    l_wu = load(wu_h, wu.at[z], 3)
    l_wd = load(
        wd_h.at[:, pl.ds(hint(core * half, half), half)],
        wd.at[core, pl.ds(hint(z * hs, hs), hs), :],
        4,
    )
    l_op = load(oproj_h, oproj, 5)
    l_res = load(resid_h, residv, 6)
    l_rt = load(routes_h, routv, 7)
    l_wt = load(wts_h, wtsv, 8)

    barrier = pltpu.get_barrier_semaphore()
    partners = []
    for i in range(1, n_sp):
        peer = lax.rem(sp + i, n_sp)
        partners += [(peer, tp), (peer, sibling)]
    for i in range(1, n_tp):
        partners.append((sp, lax.rem(tp + i, n_tp)))
    for peer in partners:
        pl.semaphore_signal(barrier, inc=1, device_id=peer, device_id_type=MESH)

    heads, hd = rg.shape[1], rg.shape[2]
    wcat[...] = jnp.zeros_like(wcat)
    for d in range(2):
        for which, ref in enumerate((rg, ig)):
            for h in range(heads):
                at = (2 * d + which) * chans + h * hd
                wcat[h * hd : (h + 1) * hd, at : at + hd] = ref[d, h]

    l_mix.wait()
    pl.semaphore_wait(barrier, len(partners))

    right = 2 * lax.rem(z + 1, nz) + core
    left = 2 * lax.rem(z + nz - 1, nz) + core

    def piece_ref(piece, shard):
        if piece == 0:
            return wg.at[shard]
        if piece == 1:
            return wu.at[shard]
        q = piece - 2
        return wd.at[:, pl.ds(hint(shard * hs, hs), hs), q * cw : (q + 1) * cw]

    def ring_copy(direction, piece, hop):
        back = (hop - 1) if direction == 0 else nz - (hop - 1)
        shard = lax.rem(z + nz - back, nz)
        dst = piece_ref(piece, shard)
        src = dst
        if hop == 1 and piece < 2:
            src = (wg_h, wu_h)[piece]
        return pltpu.make_async_remote_copy(
            src_ref=src,
            dst_ref=dst,
            send_sem=ring_send.at[direction, piece, hop - 1],
            recv_sem=ring_recv.at[direction, piece, hop - 1],
            device_id=(sp, right if direction == 0 else left),
            device_id_type=MESH,
        )

    def ring_arrived(direction, piece, hop):
        back = hop if direction == 0 else nz - hop
        shard = lax.rem(z + nz - back, nz)
        blocked_all(piece_ref(piece, shard), ring_recv.at[direction, piece, hop - 1])

    plans = ring_plan(nz)
    place = [0, 0]
    sent = []
    taken = set()

    def take(direction, piece, hop):
        if (direction, piece, hop) not in taken:
            taken.add((direction, piece, hop))
            ring_arrived(direction, piece, hop)

    def advance(count):
        for _ in range(count):
            for direction in (0, 1):
                if place[direction] < len(plans[direction]):
                    piece, hop = plans[direction][place[direction]]
                    place[direction] += 1
                    if hop > 1:
                        take(direction, piece, hop - 1)
                    ring_copy(direction, piece, hop).start()
                    sent.append((direction, piece, hop))

    def complete(piece):
        for direction in (0, 1):
            for p, hop in plans[direction]:
                if p == piece:
                    assert (direction, p, hop) in sent
                    take(direction, p, hop)

    nxt, prv = lax.rem(sp + 1, n_sp), lax.rem(sp + n_sp - 1, n_sp)
    hr = halo.shape[1]
    to_next = pltpu.make_async_remote_copy(
        src_ref=mixv.at[seq - hr : seq, :],
        dst_ref=halo.at[0],
        send_sem=halo_send.at[0],
        recv_sem=halo_recv.at[0],
        device_id=(nxt, tp),
        device_id_type=MESH,
    )
    to_prev = pltpu.make_async_remote_copy(
        src_ref=mixv.at[0:hr, :],
        dst_ref=halo.at[1],
        send_sem=halo_send.at[1],
        recv_sem=halo_recv.at[1],
        device_id=(prv, tp),
        device_id_type=MESH,
    )
    to_next.start()
    to_prev.start()

    pre = pltpu.make_async_remote_copy(
        src_ref=wd_h.at[:, pl.ds(hint(other * half, half), half)],
        dst_ref=wd.at[core, pl.ds(hint(z * hs, hs), hs), :],
        send_sem=pre_sem.at[0],
        recv_sem=pre_sem.at[1],
        device_id=(sp, sibling),
        device_id_type=MESH,
    )
    advance(2)
    pre.start()

    xpad[8 : 8 + seq, :] = mixv[...].astype(F32)
    to_next.wait()
    to_prev.wait()
    before = jnp.where(sp > 0, 1.0, 0.0).astype(F32)
    after = jnp.where(sp < n_sp - 1, 1.0, 0.0).astype(F32)
    xpad[0:8, :] = halo[0].astype(F32)[hr - 8 : hr] * before
    xpad[8 + seq : 16 + seq, :] = halo[1].astype(F32)[0:8] * after

    def strided(t):
        return xpad[pl.ds(t, SEGMENTS, stride=seg), :]

    taps = [jnp.broadcast_to(conv_w[j : j + 1, :], (SEGMENTS, chans)) for j in range(4)]
    bias = jnp.broadcast_to(conv_b[0:1, :], (SEGMENTS, chans))

    def conv_body(t, window):
        x0, x1, x2 = window
        x3 = strided(9 + t)
        conv_s[pl.ds(hint(t * SEGMENTS, SEGMENTS), SEGMENTS), :] = (
            bias + x0 * taps[0] + x1 * taps[1] + x2 * taps[2] + x3 * taps[3]
        )
        return x1, x2, x3

    lax.fori_loop(0, seg, conv_body, (strided(6), strided(7), strided(8)), unroll=8)

    rates = []
    for d in range(2):
        x = -decay[d : d + 1, :]
        rates.append(-8.0 * (jnp.maximum(x, 0.0) + jnp.log1p(jnp.exp(-jnp.abs(x)))))
    part = 128

    def coef_body(n, _):
        at = pl.ds(hint(n * part, part), part)
        c = conv_s[at, :]
        pre_act = jnp.dot(c, wcat[...], precision=HIGHEST_MODE, preferred_element_type=F32)
        for d, (a_ref, d_ref) in enumerate(((ca0, cd0), (ca1, cd1))):
            r = jax.nn.sigmoid(pre_act[:, 2 * d * chans : (2 * d + 1) * chans] + rb[d : d + 1, :])
            i = jax.nn.sigmoid(
                pre_act[:, (2 * d + 1) * chans : (2 * d + 2) * chans] + ib[d : d + 1, :]
            )
            la = r * rates[d]
            a = jnp.exp(la)
            x = 2.0 * la
            series = 1.0 + x * (1.0 / 6.0)
            for k in (5.0, 4.0, 3.0, 2.0):
                series = 1.0 + x * (1.0 / k) * series
            gap = jnp.where(x > -0.3, -x * series, 1.0 - a * a)
            a_ref[at, :] = a
            d_ref[at, :] = jnp.sqrt(gap) * (i * c)
        return 0

    lax.fori_loop(0, seq // part, coef_body, 0)

    zero = jnp.zeros((SEGMENTS, chans), F32)
    one = jnp.ones((SEGMENTS, chans), F32)

    def scan_body(t, carry):
        f, p, g, q = carry
        fat = pl.ds(hint(t * SEGMENTS, SEGMENTS), SEGMENTS)
        bat = pl.ds(hint((seg - 1 - t) * SEGMENTS, SEGMENTS), SEGMENTS)
        a, b = ca0[fat, :], ca1[bat, :]
        f = a * f + cd0[fat, :]
        p = a * p
        g = b * g + cd1[bat, :]
        q = b * q
        cd0[fat, :] = f
        ca0[fat, :] = p
        cd1[bat, :] = g
        ca1[bat, :] = q
        return f, p, g, q

    f_end, p_end, g_end, q_end = lax.fori_loop(0, seg, scan_body, (zero, one, zero, one), unroll=8)

    row = lambda v, k: v[k : k + 1, :]
    f_scale, f_shift = [row(one, 0)], [row(zero, 0)]
    for k in range(SEGMENTS):
        f_scale.append(row(p_end, k) * f_scale[-1])
        f_shift.append(row(p_end, k) * f_shift[-1] + row(f_end, k))
    b_scale, b_shift = [row(one, 0)], [row(zero, 0)]
    for k in range(SEGMENTS - 1, -1, -1):
        b_scale.append(row(q_end, k) * b_scale[-1])
        b_shift.append(row(q_end, k) * b_shift[-1] + row(g_end, k))
    for k, v in enumerate((f_scale[-1], f_shift[-1], b_scale[-1], b_shift[-1])):
        stats[sp, k : k + 1, :] = v
    for i in range(1, n_sp):
        pltpu.make_async_remote_copy(
            src_ref=stats.at[sp],
            dst_ref=stats.at[sp],
            send_sem=stat_sem.at[0],
            recv_sem=stat_sem.at[1],
            device_id=(lax.rem(sp + i, n_sp), tp),
            device_id_type=MESH,
        ).start()

    l_gate.wait()

    def gelu_body(n, _):
        at = pl.ds(hint(n * 64, 64), 64)
        xpad[at, :] = jax.nn.gelu(gatev[at, :].astype(F32))
        return 0

    lax.fori_loop(0, seq // 64, gelu_body, 0)
    blocked_all(stats.at[0 : n_sp - 1], stat_sem.at[1])

    f_in = jnp.zeros((1, chans), F32)
    b_in = jnp.zeros((1, chans), F32)
    for j in range(n_sp):
        f_in = jnp.where(j < sp, stats[j, 0:1, :] * f_in + stats[j, 1:2, :], f_in)
        k = n_sp - 1 - j
        b_in = jnp.where(k > sp, stats[k, 2:3, :] * b_in + stats[k, 3:4, :], b_in)
    f_enter = jnp.concatenate(
        [f_scale[k] * f_in + f_shift[k] for k in range(SEGMENTS)], axis=0
    )
    b_enter = jnp.concatenate(
        [b_scale[SEGMENTS - 1 - k] * b_in + b_shift[SEGMENTS - 1 - k] for k in range(SEGMENTS)],
        axis=0,
    )

    def join_body(t, _):
        at = pl.ds(hint(t * SEGMENTS, SEGMENTS), SEGMENTS)
        back = pl.ds(t, SEGMENTS, stride=seg)
        state = (cd0[at, :] + ca0[at, :] * f_enter) + (cd1[at, :] + ca1[at, :] * b_enter)
        conv_s[back, :] = state
        return 0

    lax.fori_loop(0, seg, join_body, 0, unroll=8)

    def mix_body(n, _):
        at = pl.ds(hint(n * rows, rows), rows)
        mixed[at, :] = (conv_s[at, :] * xpad[at, :]).astype(BF16)
        return 0

    lax.fori_loop(0, seq // rows, mix_body, 0)

    own_cols = pl.ds(hint(tp * chans, chans), chans)
    for i in range(1, n_tp):
        peer = lax.rem(tp + i, n_tp)
        pltpu.make_async_remote_copy(
            src_ref=mixed.at[pl.ds(hint(peer * rows, rows), rows), :],
            dst_ref=tokb.at[:, own_cols],
            send_sem=tok_sem.at[0],
            recv_sem=tok_sem.at[1],
            device_id=(sp, peer),
            device_id_type=MESH,
        ).start()
    tokb[:, own_cols] = mixed[pl.ds(own_rows, rows), :]
    advance(1)

    l_rt.wait()
    l_wt.wait()
    lane = lax.broadcasted_iota(jnp.int32, (n_sp, rows), 0)
    own_routes = routv[tp]
    own_wts = wtsv[tp]
    e0 = jnp.broadcast_to(own_routes[0:1, :], (n_sp, rows))
    e1 = jnp.broadcast_to(own_routes[1:2, :], (n_sp, rows))
    h0 = jnp.where(e0 == lane, 1.0, 0.0)
    h1 = jnp.where(e1 == lane, 1.0, 0.0)
    earlier = jnp.where(
        lax.broadcasted_iota(jnp.int32, (rows, rows), 0)
        < lax.broadcasted_iota(jnp.int32, (rows, rows), 1),
        1.0,
        0.0,
    )
    counts = jnp.dot(
        (h0 + h1).astype(BF16), earlier.astype(BF16), preferred_element_type=F32
    )
    slot0 = jnp.sum(counts * h0, axis=0, keepdims=True).astype(jnp.int32) + own_routes[
        0:1, :
    ] * cap
    slot1 = jnp.sum(counts * h1, axis=0, keepdims=True).astype(jnp.int32) + own_routes[
        1:2, :
    ] * cap
    slot_id = lax.broadcasted_iota(jnp.int32, (slots, rows), 0)
    hit0, hit1 = slot_id == slot0, slot_id == slot1
    sel = jnp.where(hit0 | hit1, 1.0, 0.0).astype(BF16)
    weights = jnp.where(hit0, own_wts[0:1, :], 0.0) + jnp.where(hit1, own_wts[1:2, :], 0.0)
    eye = jnp.where(
        lax.broadcasted_iota(jnp.int32, (rows, rows), 0)
        == lax.broadcasted_iota(jnp.int32, (rows, rows), 1),
        1.0,
        0.0,
    )
    table = lax.dot_general(
        eye,
        weights,
        (((1,), (1,)), ((), ())),
        precision=HIGHEST_MODE,
        preferred_element_type=F32,
    )
    high = table.astype(BF16)
    wtab[0] = high
    wtab[1] = (table - high.astype(F32)).astype(BF16)

    l_op.wait()
    l_res.wait()
    blocked_all(tokb.at[:, 0 : (n_tp - 1) * chans], tok_sem.at[1])
    advance(1)
    pw = min(512, width)

    def proj_body(n, _):
        at = pl.ds(hint(n * pw, pw), pw)
        pbuf[:, at] = (
            jnp.dot(tokb[...], oproj[:, at], preferred_element_type=F32).astype(BF16).astype(F32)
        )
        return 0

    lax.fori_loop(0, width // pw, proj_body, 0)

    def norm_body(n, _):
        at = pl.ds(hint(n * 16, 16), 16)
        v = pbuf[at, :]
        s = (residv[at, :].astype(F32) + v * root_mean(v) * gain[0:1, :]).astype(BF16).astype(F32)
        stream_s[at, :] = s
        normed[at, :] = (s * root_mean(s) * gain[1:2, :]).astype(BF16)
        return 0

    lax.fori_loop(0, rows // 16, norm_body, 0)

    gw = min(256, width)

    def dispatch_body(n, _):
        at = pl.ds(hint(n * gw, gw), gw)
        outg[:, at] = jnp.dot(sel, normed[:, at], preferred_element_type=F32).astype(BF16)
        return 0

    lax.fori_loop(0, width // gw, dispatch_body, 0)
    own_slots = pl.ds(hint(sp * cap, cap), cap)
    for i in range(1, n_sp):
        peer = lax.rem(sp + i, n_sp)
        pltpu.make_async_remote_copy(
            src_ref=outg.at[pl.ds(hint(peer * cap, cap), cap), :],
            dst_ref=arr.at[core, own_slots, :],
            send_sem=disp_send.at[0],
            recv_sem=disp_recv.at[i - 1],
            device_id=(peer, tp),
            device_id_type=MESH,
        ).start()

    def forward(src_ref, at):
        pltpu.make_async_remote_copy(
            src_ref=src_ref,
            dst_ref=arr.at[core, at, :],
            send_sem=fwd_sem.at[0],
            recv_sem=fwd_sem.at[1],
            device_id=(sp, sibling),
            device_id_type=MESH,
        ).start()

    forward(outg.at[own_slots, :], own_slots)
    arr[core, own_slots, :] = outg[own_slots, :]
    advance(1)
    for i in range(1, n_sp):
        src = lax.rem(sp + n_sp - i, n_sp)
        at = pl.ds(hint(src * cap, cap), cap)
        blocked_all(arr.at[core, at, :], disp_recv.at[i - 1])
        forward(arr.at[core, at, :], at)
        if i == n_sp // 2:
            advance(1)

    while not all(
        any(ev == (p, h) for ev in plans[d][: place[d]])
        for d in (0, 1)
        for p, h in plans[d]
        if p < 2
    ):
        advance(1)
    l_wg.wait()
    l_wu.wait()
    l_wd.wait()
    pre.wait()
    advance(2)
    blocked_all(arr.at[other], fwd_sem.at[1])
    complete(0)
    complete(1)
    advance(2)
    hidden_all = nz * hs
    hw = min(256, hidden_all)
    hm = min(256, slots)
    zh = hw // hs
    per = slots // hm

    def gate_body(n, _):
        c, m = n // per, lax.rem(n, per)
        at = pl.ds(hint(m * hm, hm), hm)
        x = arr[c, at, :]
        for k in range(hidden_all // hw):
            dims = (((1,), (1,)), ((), ()))
            g = lax.dot_general(
                x,
                wg[k * zh : (k + 1) * zh].reshape(hw, width),
                dims,
                preferred_element_type=F32,
            )
            u = lax.dot_general(
                x,
                wu[k * zh : (k + 1) * zh].reshape(hw, width),
                dims,
                preferred_element_type=F32,
            )
            hid[core, pl.ds(hint(n * hm, hm), hm), k * hw : (k + 1) * hw] = (
                g * jax.nn.sigmoid(g) * u
            ).astype(BF16)
        return 0

    lax.fori_loop(0, 2 * per, gate_body, 0)
    swap = pltpu.make_async_remote_copy(
        src_ref=hid.at[core],
        dst_ref=hid.at[core],
        send_sem=hid_sem.at[0],
        recv_sem=hid_sem.at[1],
        device_id=(sp, sibling),
        device_id_type=MESH,
    )
    swap.start()
    advance(1)
    swap.wait_recv()

    for q in range(CHUNKS):
        while not all(
            any(ev == (p, h) for ev in plans[d][: place[d]])
            for d in (0, 1)
            for p, h in plans[d]
            if p == 2 + q
        ):
            advance(1)
        advance(1)
        complete(2 + q)

        def down_body(n, _):
            at = pl.ds(hint(n * hm, hm), hm)
            o = jnp.dot(
                hid[0, at, :], wd[0, :, q * cw : (q + 1) * cw], preferred_element_type=F32
            ) + jnp.dot(hid[1, at, :], wd[1, :, q * cw : (q + 1) * cw], preferred_element_type=F32)
            outb[q, at, :] = o.astype(BF16)
            return 0

        lax.fori_loop(0, 2 * per, down_body, 0)
        for i in range(n_sp):
            peer = lax.rem(sp + i, n_sp)
            for mine in (1, 0):
                if i == 0 and mine:
                    continue
                c = core if mine else other
                pltpu.make_async_remote_copy(
                    src_ref=outb.at[q, pl.ds(hint(c * slots + peer * cap, cap), cap), :],
                    dst_ref=ret.at[core, q, own_slots, :],
                    send_sem=ret_send.at[q, mine],
                    recv_sem=ret_recv.at[q, mine],
                    device_id=(peer, tp if mine else sibling),
                    device_id_type=MESH,
                ).start()
        ret[core, q, own_slots, :] = outb[
            q, pl.ds(hint(core * slots + sp * cap, cap), cap), :
        ]

    for q in range(CHUNKS):
        blocked_all(ret.at[core, q, 0 : slots - cap, :], ret_recv.at[q, 1])
        blocked_all(ret.at[other, q], ret_recv.at[q, 0])
        for c in range(2):
            v = ret[c, q]
            o = jnp.dot(wtab[0], v, preferred_element_type=F32) + jnp.dot(
                wtab[1], v, preferred_element_type=F32
            )
            pbuf[:, c * half + q * cw : c * half + (q + 1) * cw] = o.astype(BF16).astype(F32)

    def final_body(n, _):
        at = pl.ds(hint(n * 16, 16), 16)
        v = pbuf[at, :]
        out_ref[at, :] = (stream_s[at, :] + v * root_mean(v) * gain[2:3, :]).astype(BF16)
        return 0

    lax.fori_loop(0, rows // 16, final_body, 0)

    blocked_all(stats.at[0 : n_sp - 1], stat_sem.at[0])
    blocked_all(tokb.at[:, 0 : (n_tp - 1) * chans], tok_sem.at[0])
    blocked_all(outg.at[0 : slots - cap, :], disp_send.at[0])
    blocked_all(outg, fwd_sem.at[0])
    swap.wait_send()
    for q in range(CHUNKS):
        blocked_all(ret.at[core, q, 0 : slots - cap, :], ret_send.at[q, 1])
        blocked_all(ret.at[other, q], ret_send.at[q, 0])
    for event in sent:
        ring_copy(*event).wait_send()


def on_device(
    mix_in,
    gate_in,
    conv_w,
    conv_b,
    decay_param,
    recur_gate,
    recur_bias,
    input_gate,
    input_bias,
    residual,
    out_proj,
    norm_gain,
    routes,
    route_wt,
    exp_gate,
    exp_up,
    exp_down,
):
    n_sp, n_tp = lax.axis_size("sp"), lax.axis_size("tp")
    nz = n_tp // 2
    seq, chans = mix_in.shape
    rows, width = residual.shape
    top = routes.shape[1]
    experts = n_sp * exp_gate.shape[0]
    cap = 2 * rows * top // experts
    slots = experts * cap
    hs = exp_gate.shape[2]
    half = width // 2
    far = nz // 2
    pieces = 2 + CHUNKS

    def tables(array):
        return array.T.reshape(top, n_tp, rows).transpose(1, 0, 2)

    anywhere = pl.BlockSpec(memory_space=pl.ANY)
    onchip = pl.BlockSpec(memory_space=pltpu.VMEM)
    dma = pltpu.SemaphoreType.DMA
    scratch = [
        pltpu.VMEM((seq, chans), BF16),
        pltpu.VMEM((seq, chans), BF16),
        pltpu.VMEM((rows, width), BF16),
        pltpu.VMEM(out_proj.shape, BF16),
        pltpu.VMEM((n_tp, top, rows), jnp.int32),
        pltpu.VMEM((n_tp, top, rows), F32),
        pltpu.VMEM((2, 16, chans), BF16),
        pltpu.VMEM((seq + 16, chans), F32),
        pltpu.VMEM((seq, chans), F32),
        pltpu.VMEM((chans, 4 * chans), F32),
        pltpu.VMEM((seq, chans), F32),
        pltpu.VMEM((seq, chans), F32),
        pltpu.VMEM((seq, chans), F32),
        pltpu.VMEM((seq, chans), F32),
        pltpu.VMEM((n_sp, 8, chans), F32),
        pltpu.VMEM((seq, chans), BF16),
        pltpu.VMEM((rows, n_tp * chans), BF16),
        pltpu.VMEM((rows, width), F32),
        pltpu.VMEM((rows, width), F32),
        pltpu.VMEM((rows, width), BF16),
        pltpu.VMEM((slots, width), BF16),
        pltpu.VMEM((2, slots, width), BF16),
        pltpu.VMEM((nz, hs, width), BF16),
        pltpu.VMEM((nz, hs, width), BF16),
        pltpu.VMEM((2, nz * hs, half), BF16),
        pltpu.VMEM((2, 2 * slots, nz * hs), BF16),
        pltpu.VMEM((CHUNKS, 2 * slots, half // CHUNKS), BF16),
        pltpu.VMEM((2, CHUNKS, slots, half // CHUNKS), BF16),
        pltpu.VMEM((2, rows, slots), BF16),
        dma((9,)),
        dma((2,)),
        dma((2,)),
        dma((2,)),
        dma((2,)),
        dma((1,)),
        dma((n_sp - 1,)),
        dma((2,)),
        dma((2,)),
        dma((2,)),
        dma((2, pieces, far)),
        dma((2, pieces, far)),
        dma((CHUNKS, 2)),
        dma((CHUNKS, 2)),
    ]
    where = [
        anywhere,
        anywhere,
        onchip,
        onchip,
        onchip,
        onchip,
        onchip,
        onchip,
        onchip,
        anywhere,
        anywhere,
        onchip,
        anywhere,
        anywhere,
        anywhere,
        anywhere,
        anywhere,
    ]
    return pl.pallas_call(
        functools.partial(kernel, n_sp, n_tp),
        out_shape=jax.ShapeDtypeStruct((rows, width), BF16),
        in_specs=where,
        out_specs=onchip,
        scratch_shapes=scratch,
        compiler_params=pltpu.CompilerParams(
            collective_id=0, has_side_effects=True, vmem_limit_bytes=60 * 1024 * 1024
        ),
    )(
        mix_in,
        gate_in,
        conv_w,
        conv_b.reshape(1, chans),
        decay_param,
        recur_gate,
        recur_bias,
        input_gate,
        input_bias,
        residual,
        out_proj,
        norm_gain,
        tables(routes),
        tables(route_wt),
        exp_gate[0].T,
        exp_up[0].T,
        exp_down[0],
    )


def solution(mesh):
    return jax.shard_map(
        on_device,
        mesh=mesh,
        in_specs=(
            P("sp", "tp"),
            P("sp", "tp"),
            P(None, "tp"),
            P("tp"),
            P(None, "tp"),
            P(None, "tp", None, None),
            P(None, "tp"),
            P(None, "tp", None, None),
            P(None, "tp"),
            P(("sp", "tp"), None),
            P(),
            P(),
            P("sp", None),
            P("sp", None),
            P("sp", None, "tp"),
            P("sp", None, "tp"),
            P("sp", "tp", None),
        ),
        out_specs=P(("sp", "tp"), None),
        check_vma=False,
    )
```

time: 249 us -> 107 us (0.43)
  Pallas kernels: 0 us -> 103 us
  local copies, waits for them, and re-layouts: 71.7 us -> 4.45 us
  other arithmetic: 52.7 us -> 0 us
  starting transfers between devices: 34.9 us -> 0 us
  waiting for transfers between devices: 31.2 us -> 0 us
  matrix products: 21.8 us -> 0 us
  blocking collectives: 19.8 us -> 0 us
  between operations: 14.9 us -> 0.01 us
    pallas_call x0 -> x1, Pallas kernels: none -> 103 us  [on_device(): pl.pallas_call(functools.partial(kernel, n_sp, n_tp), out_shape=jax.Shape...]
    slice x175 -> x0, local copies, waits for them, and re-layouts: 49.1 us -> none  [the longest x74 26 us: on_device(): lax.associative_scan(pair_join, (jnp.flip(bwd_decay, 0), jnp.flip(bwd_dri...]
    all_to_all x4 -> x0, waiting for transfers between devices: 31.1 us -> none  [the longest x1 15 us: on_device(): lax.all_to_all(out_rows, 'sp', split_axis=1, concat_axis=0, tiled=True)]
    all_to_all x4 -> x0, starting transfers between devices: 29.6 us -> none  [the longest x2 14.3 us: copy_for_each(): return lax.all_to_all(copies, axis, split_axis=0, concat_axis=0, tiled=True)]
    concatenate x39 -> x0, other arithmetic: 25.4 us -> none  [the longest x18 12.9 us: on_device(): lax.associative_scan(pair_join, (jnp.flip(bwd_decay, 0), jnp.flip(bwd_dri...]
    dot_general x9 -> x0, matrix products: 21.8 us -> none  [the longest x1 6.93 us: on_device(): jnp.einsum('emf,efd->emd', hidden, lax.all_gather(exp_down, 'tp', axis=1,...]
    all_to_all x1 -> x0, blocking collectives: 19.8 us -> none  [on_device(): lax.all_to_all(outgoing.reshape(experts, capacity, width_model), 'sp', sp...]
    add x79 -> x0, other arithmetic: 19.5 us -> none  [the longest x36 12.6 us: pair_join(): later_pair[0] * earlier[1] + later_pair[1]]
  transfers between devices with their start and end apart: 8 -> 0, of which waited for: 3 -> 0; matrix products, arithmetic and copies ran while one was open for 55% -> 0% of each run, Pallas kernels for 0% -> 0%
where the time goes in v1:
time: 107 us
  Pallas kernels  103 us (96%)
  local copies, waits for them, and re-layouts  4.45 us (4%)
    pallas_call x1, Pallas kernels, on_device(): pl.pallas_call(functools.partial(kernel, n_sp, n_tp), out_shape=jax.Shape...  103 us
    reshape x4, local copies, waits for them, and re-layouts, tables(): return array.T.reshape(top, n_tp, rows).transpose(1, 0, 2)  2.78 us

profile of v1, /device:TPU:1, one launch (start us, length us, event | category | flops | bytes accessed | tf_op | source)
XLA Modules:
  0.0 107.1 jit_solution(8656761200151273558)
XLA Ops:
  0.0 0.8 reshape.10
  0.8 0.6 copy.23
  1.4 0.8 reshape.11
  2.2 0.6 copy.22
  2.8 102.7 %shard_map.163 = bf16[64,2048]{1,0:T(8,128)(2,1)} custom-call(bf16[1024,128]{1,0:T(8,128)(2,1)} %mix_h.1, bf16[1024,128]{1,0:T(8,128)(2,1)} %gate_h.1, f32[4,128]{1,0:T(4,128)} %conv_w.1, f32[1,128]{1,0:T(1,128)} %bitcast.23, f32[2,128]{1,0:T(2,128)} %decay.1, f32[2,2,64,64]{3,2,1,0:T(8,128)} %rg.1, f32[2,128]{1,0:T(2,128)} %rb.1, f32[2,2,64,64]{3,2,1,0:T(8,128)} %ig.1, ...), custom_call_target="tpu_custom_call" | custom-call | tf_op jit(solution)/shard_map/pallas_call | solution.py:745
  105.4 1.7 %copy.25 = bf16[64,2048]{1,0:T(8,128)(2,1)} copy(bf16[64,2048]{1,0:T(8,128)(2,1)} %shard_map.163) | data formatting | bytes 524288

commit v2 on v1

--- a/solution.py
+++ b/solution.py
@@ -12,7 +12,78 @@
 MESH = pl.DeviceIdType.MESH
 F32, BF16 = jnp.float32, jnp.bfloat16
 SEGMENTS = 8
-CHUNKS = 4
+WIDTHS = (128, 128, 128, 128, 256, 256)
+CHUNKS = len(WIDTHS)
+NEVER = 1 << 20
+PLAN = (
+    ((0, 0, 1), (0, 1, 1), (1, 1, 1), (1, 0, 1),),
+    (),
+    ((0, 4, 1), (0, 5, 1), (0, 2, 1), (0, 3, 1), (1, 4, 1), (1, 5, 1), (1, 2, 1), (1, 3, 1),),
+    (),
+    (),
+    (),
+    ((0, 0, 2), (1, 1, 2),),
+    (),
+    ((0, 1, 2), (1, 0, 2), (0, 0, 3), (1, 2, 2), (1, 1, 3),),
+    (),
+    (),
+    (),
+    (),
+    (),
+    ((0, 2, 2), (0, 3, 2), (0, 4, 2), (0, 5, 2), (0, 6, 1), (1, 3, 2), (1, 4, 2), (1, 5, 2), (1, 6, 1), (0, 1, 3), (1, 7, 1), (1, 2, 3),),
+    (),
+    ((1, 0, 3),),
+    (),
+    (),
+    (),
+    (),
+    ((0, 2, 3),),
+    ((0, 3, 3), (1, 3, 3),),
+    (),
+    (),
+    ((0, 0, 4), (1, 1, 4),),
+    (),
+    (),
+    (),
+    (),
+    ((0, 6, 2), (0, 7, 1), (0, 4, 3), (1, 6, 2), (1, 7, 2),),
+    (),
+    ((0, 2, 4), (1, 3, 4),),
+    ((0, 6, 3), (1, 4, 3),),
+    ((1, 5, 3),),
+    ((0, 4, 4), (1, 6, 3),),
+    ((0, 7, 2),),
+    (),
+    (),
+    (),
+    ((1, 7, 3),),
+    (),
+    (),
+    (),
+    ((0, 5, 3),),
+    (),
+    (),
+    (),
+    ((0, 6, 4), (1, 5, 4),),
+    (),
+    (),
+    (),
+    (),
+    ((0, 7, 3), (1, 7, 4),),
+    (),
+    (),
+    (),
+    (),
+    (),
+    (),
+    (),
+    (),
+    (),
+    (),
+    (),
+    (),
+)
+STARTS = tuple(sum(WIDTHS[:k]) for k in range(CHUNKS))
 
 
 def hint(value, step):
@@ -27,21 +98,11 @@
     return lax.rsqrt(jnp.mean(values * values, axis=-1, keepdims=True) + EPSILON)
 
 
-def ring_plan(nz):
-    far, near = nz // 2, nz - 1 - nz // 2
-    plans = []
-    for direction in (0, 1):
-        hops = lambda piece: far if (piece % 2 == direction) else near
-        order = []
-        groups = [(0, 1)] + [(2 + 2 * k, 3 + 2 * k) for k in range(CHUNKS // 2)]
-        for group in groups:
-            first = group if direction == 0 else group[::-1]
-            for hop in range(1, far + 1):
-                for piece in first:
-                    if hop <= hops(piece):
-                        order.append((piece, hop))
-        plans.append(order)
-    return plans
+def places(nz):
+    order = [0]
+    for step in range(1, nz // 2 + 1):
+        order += [step, nz - step] if step < nz - step else [step]
+    return {distance: place for place, distance in enumerate(order)}
 
 
 def kernel(
@@ -102,7 +163,8 @@
     disp_send,
     disp_recv,
     fwd_sem,
-    hid_sem,
+    hid_send,
+    hid_recv,
     pre_sem,
     ring_send,
     ring_recv,
@@ -121,27 +183,35 @@
     cap = outg.shape[0] // n_sp
     slots = n_sp * cap
     seg = seq // SEGMENTS
-    cw = half // CHUNKS
+
+    loads = {}
+    drains = []
 
     def load(src, dst, k):
         copy = pltpu.make_async_copy(src, dst, load_sem.at[k])
         copy.start()
-        return copy
+        loads[k] = copy
+        return k
+
+    def need(k):
+        if k in loads:
+            loads.pop(k).wait()
 
     own_rows = hint(tp * rows, rows)
     l_mix = load(mix_h, mixv, 0)
     l_gate = load(gate_h, gatev, 1)
-    l_wg = load(wg_h, wg.at[z], 2)
-    l_wu = load(wu_h, wu.at[z], 3)
+    l_wg = load(wg_h, wg.at[0], 2)
+    l_wu = load(wu_h, wu.at[0], 3)
     l_wd = load(
         wd_h.at[:, pl.ds(hint(core * half, half), half)],
-        wd.at[core, pl.ds(hint(z * hs, hs), hs), :],
+        wd.at[core, 0:hs, :],
         4,
     )
     l_op = load(oproj_h, oproj, 5)
     l_res = load(resid_h, residv, 6)
-    l_rt = load(routes_h, routv, 7)
-    l_wt = load(wts_h, wtsv, 8)
+    pair = pl.ds(hint(z * 2 * rows, 2 * rows), 2 * rows)
+    l_rt = load(routes_h.at[:, pair], routv, 7)
+    l_wt = load(wts_h.at[:, pair], wtsv, 8)
 
     barrier = pltpu.get_barrier_semaphore()
     partners = []
@@ -161,68 +231,73 @@
                 at = (2 * d + which) * chans + h * hd
                 wcat[h * hd : (h + 1) * hd, at : at + hd] = ref[d, h]
 
-    l_mix.wait()
+    need(l_mix)
     pl.semaphore_wait(barrier, len(partners))
 
     right = 2 * lax.rem(z + 1, nz) + core
     left = 2 * lax.rem(z + nz - 1, nz) + core
 
-    def piece_ref(piece, shard):
-        if piece == 0:
-            return wg.at[shard]
-        if piece == 1:
-            return wu.at[shard]
+    far, near = nz // 2, nz - 1 - nz // 2
+    place = places(nz)
+
+    def hops(direction, piece):
+        return far if piece % 2 == direction else near
+
+    def piece_ref(direction, piece, hop):
+        at = place[hop if direction == 1 or hop == 0 else nz - hop]
+        if piece < 2:
+            return (wg, wu)[piece].at[at]
         q = piece - 2
-        return wd.at[:, pl.ds(hint(shard * hs, hs), hs), q * cw : (q + 1) * cw]
+        return wd.at[:, at * hs : (at + 1) * hs, STARTS[q] : STARTS[q] + WIDTHS[q]]
 
     def ring_copy(direction, piece, hop):
-        back = (hop - 1) if direction == 0 else nz - (hop - 1)
-        shard = lax.rem(z + nz - back, nz)
-        dst = piece_ref(piece, shard)
-        src = dst
+        src = piece_ref(direction, piece, hop - 1)
         if hop == 1 and piece < 2:
             src = (wg_h, wu_h)[piece]
         return pltpu.make_async_remote_copy(
             src_ref=src,
-            dst_ref=dst,
+            dst_ref=piece_ref(direction, piece, hop),
             send_sem=ring_send.at[direction, piece, hop - 1],
             recv_sem=ring_recv.at[direction, piece, hop - 1],
             device_id=(sp, right if direction == 0 else left),
             device_id_type=MESH,
         )
 
-    def ring_arrived(direction, piece, hop):
-        back = hop if direction == 0 else nz - hop
-        shard = lax.rem(z + nz - back, nz)
-        blocked_all(piece_ref(piece, shard), ring_recv.at[direction, piece, hop - 1])
-
-    plans = ring_plan(nz)
-    place = [0, 0]
     sent = []
     taken = set()
+    stage = [0]
 
     def take(direction, piece, hop):
         if (direction, piece, hop) not in taken:
             taken.add((direction, piece, hop))
-            ring_arrived(direction, piece, hop)
-
-    def advance(count):
-        for _ in range(count):
-            for direction in (0, 1):
-                if place[direction] < len(plans[direction]):
-                    piece, hop = plans[direction][place[direction]]
-                    place[direction] += 1
-                    if hop > 1:
-                        take(direction, piece, hop - 1)
-                    ring_copy(direction, piece, hop).start()
-                    sent.append((direction, piece, hop))
-
-    def complete(piece):
+            blocked_all(
+                piece_ref(direction, piece, hop), ring_recv.at[direction, piece, hop - 1]
+            )
+
+    def poll():
+        for direction, piece, hop in PLAN[stage[0]]:
+            if hop > 1:
+                take(direction, piece, hop - 1)
+            elif piece >= 2 and "pre" not in taken:
+                taken.add("pre")
+                need(l_wd)
+                pre.wait()
+            ring_copy(direction, piece, hop).start()
+            sent.append((direction, piece, hop))
+        stage[0] += 1
+
+    def complete(piece, end=NEVER):
         for direction in (0, 1):
-            for p, hop in plans[direction]:
-                if p == piece:
-                    assert (direction, p, hop) in sent
-                    take(direction, p, hop)
+            for hop in range(1, hops(direction, piece) + 1):
+                if place[hop if direction == 1 else nz - hop] < end:
+                    assert (direction, piece, hop) in sent
+                    take(direction, piece, hop)
+
+    def finish():
+        for drain in drains:
+            drain()
+        for event in sent:
+            ring_copy(*event).wait_send()
 
     nxt, prv = lax.rem(sp + 1, n_sp), lax.rem(sp + n_sp - 1, n_sp)
     hr = halo.shape[1]
@@ -247,35 +322,32 @@
 
     pre = pltpu.make_async_remote_copy(
         src_ref=wd_h.at[:, pl.ds(hint(other * half, half), half)],
-        dst_ref=wd.at[core, pl.ds(hint(z * hs, hs), hs), :],
+        dst_ref=wd.at[core, 0:hs, :],
         send_sem=pre_sem.at[0],
         recv_sem=pre_sem.at[1],
         device_id=(sp, sibling),
         device_id_type=MESH,
     )
-    advance(2)
+    poll()
     pre.start()
 
+    xpad[0:8, :] = jnp.zeros((8, chans), F32)
     xpad[8 : 8 + seq, :] = mixv[...].astype(F32)
-    to_next.wait()
-    to_prev.wait()
-    before = jnp.where(sp > 0, 1.0, 0.0).astype(F32)
-    after = jnp.where(sp < n_sp - 1, 1.0, 0.0).astype(F32)
-    xpad[0:8, :] = halo[0].astype(F32)[hr - 8 : hr] * before
-    xpad[8 + seq : 16 + seq, :] = halo[1].astype(F32)[0:8] * after
+    xpad[8 + seq : 16 + seq, :] = jnp.zeros((8, chans), F32)
 
     def strided(t):
         return xpad[pl.ds(t, SEGMENTS, stride=seg), :]
 
     taps = [jnp.broadcast_to(conv_w[j : j + 1, :], (SEGMENTS, chans)) for j in range(4)]
     bias = jnp.broadcast_to(conv_b[0:1, :], (SEGMENTS, chans))
+
+    def weigh(x0, x1, x2, x3):
+        return bias + x0 * taps[0] + x1 * taps[1] + x2 * taps[2] + x3 * taps[3]
 
     def conv_body(t, window):
         x0, x1, x2 = window
         x3 = strided(9 + t)
-        conv_s[pl.ds(hint(t * SEGMENTS, SEGMENTS), SEGMENTS), :] = (
-            bias + x0 * taps[0] + x1 * taps[1] + x2 * taps[2] + x3 * taps[3]
-        )
+        conv_s[pl.ds(hint(t * SEGMENTS, SEGMENTS), SEGMENTS), :] = weigh(x0, x1, x2, x3)
         return x1, x2, x3
 
     lax.fori_loop(0, seg, conv_body, (strided(6), strided(7), strided(8)), unroll=8)
@@ -286,11 +358,10 @@
         rates.append(-8.0 * (jnp.maximum(x, 0.0) + jnp.log1p(jnp.exp(-jnp.abs(x)))))
     part = 128
 
-    def coef_body(n, _):
-        at = pl.ds(hint(n * part, part), part)
-        c = conv_s[at, :]
+    def coefficients(c):
         pre_act = jnp.dot(c, wcat[...], precision=HIGHEST_MODE, preferred_element_type=F32)
-        for d, (a_ref, d_ref) in enumerate(((ca0, cd0), (ca1, cd1))):
+        found = []
+        for d in range(2):
             r = jax.nn.sigmoid(pre_act[:, 2 * d * chans : (2 * d + 1) * chans] + rb[d : d + 1, :])
             i = jax.nn.sigmoid(
                 pre_act[:, (2 * d + 1) * chans : (2 * d + 2) * chans] + ib[d : d + 1, :]
@@ -302,11 +373,34 @@
             for k in (5.0, 4.0, 3.0, 2.0):
                 series = 1.0 + x * (1.0 / k) * series
             gap = jnp.where(x > -0.3, -x * series, 1.0 - a * a)
-            a_ref[at, :] = a
-            d_ref[at, :] = jnp.sqrt(gap) * (i * c)
+            found += [a, jnp.sqrt(gap) * (i * c)]
+        return found
+
+    kept = (ca0, cd0, ca1, cd1)
+
+    def coef_body(n, _):
+        at = pl.ds(hint(n * part, part), part)
+        for ref, value in zip(kept, coefficients(conv_s[at, :])):
+            ref[at, :] = value
         return 0
 
-    lax.fori_loop(0, seq // part, coef_body, 0)
+    lax.fori_loop(0, seq // part // 2, coef_body, 0)
+    poll()
+    lax.fori_loop(seq // part // 2, seq // part, coef_body, 0)
+
+    poll()
+    to_next.wait()
+    to_prev.wait()
+    before = jnp.where(sp > 0, 1.0, 0.0).astype(F32)
+    after = jnp.where(sp < n_sp - 1, 1.0, 0.0).astype(F32)
+    xpad[0:8, :] = halo[0].astype(F32)[hr - 8 : hr] * before
+    xpad[8 + seq : 16 + seq, :] = halo[1].astype(F32)[0:8] * after
+    ends = jnp.concatenate(
+        [weigh(*(strided(6 + t + j) for j in range(4))) for t in (0, 1, seg - 1)], axis=0
+    )
+    for ref, value in zip(kept, coefficients(ends)):
+        ref[0 : 2 * SEGMENTS, :] = value[0 : 2 * SEGMENTS]
+        ref[seq - SEGMENTS : seq, :] = value[2 * SEGMENTS :]
 
     zero = jnp.zeros((SEGMENTS, chans), F32)
     one = jnp.ones((SEGMENTS, chans), F32)
@@ -327,6 +421,8 @@
         return f, p, g, q
 
     f_end, p_end, g_end, q_end = lax.fori_loop(0, seg, scan_body, (zero, one, zero, one), unroll=8)
+
+    poll()
 
     row = lambda v, k: v[k : k + 1, :]
     f_scale, f_shift = [row(one, 0)], [row(zero, 0)]
@@ -348,8 +444,10 @@
             device_id=(lax.rem(sp + i, n_sp), tp),
             device_id_type=MESH,
         ).start()
-
-    l_gate.wait()
+    drains.append(lambda: blocked_all(stats.at[0 : n_sp - 1], stat_sem.at[0]))
+    poll()
+
+    need(l_gate)
 
     def gelu_body(n, _):
         at = pl.ds(hint(n * 64, 64), 64)
@@ -357,6 +455,7 @@
         return 0
 
     lax.fori_loop(0, seq // 64, gelu_body, 0)
+    poll()
     blocked_all(stats.at[0 : n_sp - 1], stat_sem.at[1])
 
     f_in = jnp.zeros((1, chans), F32)
@@ -388,6 +487,7 @@
         return 0
 
     lax.fori_loop(0, seq // rows, mix_body, 0)
+    poll()
 
     own_cols = pl.ds(hint(tp * chans, chans), chans)
     for i in range(1, n_tp):
@@ -400,14 +500,15 @@
             device_id=(sp, peer),
             device_id_type=MESH,
         ).start()
+    drains.append(lambda: blocked_all(tokb.at[:, 0 : (n_tp - 1) * chans], tok_sem.at[0]))
     tokb[:, own_cols] = mixed[pl.ds(own_rows, rows), :]
-    advance(1)
-
-    l_rt.wait()
-    l_wt.wait()
+    poll()
+
+    need(l_rt)
+    need(l_wt)
     lane = lax.broadcasted_iota(jnp.int32, (n_sp, rows), 0)
-    own_routes = routv[tp]
-    own_wts = wtsv[tp]
+    own_routes = jnp.where(core == 0, routv[:, 0:rows], routv[:, rows : 2 * rows])
+    own_wts = jnp.where(core == 0, wtsv[:, 0:rows], wtsv[:, rows : 2 * rows])
     e0 = jnp.broadcast_to(own_routes[0:1, :], (n_sp, rows))
     e1 = jnp.broadcast_to(own_routes[1:2, :], (n_sp, rows))
     h0 = jnp.where(e0 == lane, 1.0, 0.0)
@@ -448,10 +549,11 @@
     wtab[0] = high
     wtab[1] = (table - high.astype(F32)).astype(BF16)
 
-    l_op.wait()
-    l_res.wait()
+    need(l_op)
+    need(l_res)
+    poll()
     blocked_all(tokb.at[:, 0 : (n_tp - 1) * chans], tok_sem.at[1])
-    advance(1)
+    poll()
     pw = min(512, width)
 
     def proj_body(n, _):
@@ -462,6 +564,7 @@
         return 0
 
     lax.fori_loop(0, width // pw, proj_body, 0)
+    poll()
 
     def norm_body(n, _):
         at = pl.ds(hint(n * 16, 16), 16)
@@ -472,6 +575,7 @@
         return 0
 
     lax.fori_loop(0, rows // 16, norm_body, 0)
+    poll()
 
     gw = min(256, width)
 
@@ -481,6 +585,7 @@
         return 0
 
     lax.fori_loop(0, width // gw, dispatch_body, 0)
+    poll()
     own_slots = pl.ds(hint(sp * cap, cap), cap)
     for i in range(1, n_sp):
         peer = lax.rem(sp + i, n_sp)
@@ -493,6 +598,8 @@
             device_id_type=MESH,
         ).start()
 
+    drains.append(lambda: blocked_all(outg.at[0 : slots - cap, :], disp_send.at[0]))
+
     def forward(src_ref, at):
         pltpu.make_async_remote_copy(
             src_ref=src_ref,
@@ -504,94 +611,89 @@
         ).start()
 
     forward(outg.at[own_slots, :], own_slots)
+    drains.append(lambda: blocked_all(outg, fwd_sem.at[0]))
     arr[core, own_slots, :] = outg[own_slots, :]
-    advance(1)
+    poll()
     for i in range(1, n_sp):
         src = lax.rem(sp + n_sp - i, n_sp)
         at = pl.ds(hint(src * cap, cap), cap)
         blocked_all(arr.at[core, at, :], disp_recv.at[i - 1])
         forward(arr.at[core, at, :], at)
-        if i == n_sp // 2:
-            advance(1)
-
-    while not all(
-        any(ev == (p, h) for ev in plans[d][: place[d]])
-        for d in (0, 1)
-        for p, h in plans[d]
-        if p < 2
-    ):
-        advance(1)
-    l_wg.wait()
-    l_wu.wait()
-    l_wd.wait()
-    pre.wait()
-    advance(2)
-    blocked_all(arr.at[other], fwd_sem.at[1])
-    complete(0)
-    complete(1)
-    advance(2)
+        poll()
+
     hidden_all = nz * hs
     hw = min(256, hidden_all)
-    hm = min(256, slots)
     zh = hw // hs
-    per = slots // hm
-
-    def gate_body(n, _):
-        c, m = n // per, lax.rem(n, per)
-        at = pl.ds(hint(m * hm, hm), hm)
-        x = arr[c, at, :]
-        for k in range(hidden_all // hw):
-            dims = (((1,), (1,)), ((), ()))
-            g = lax.dot_general(
+    dims = (((1,), (1,)), ((), ()))
+
+    def swap(c, k):
+        at = hid.at[core, pl.ds(hint(c * slots, slots), slots), k * hw : (k + 1) * hw]
+        return pltpu.make_async_remote_copy(
+            src_ref=at,
+            dst_ref=at,
+            send_sem=hid_send.at[c, k],
+            recv_sem=hid_recv.at[c, k],
+            device_id=(sp, sibling),
+            device_id_type=MESH,
+        )
+
+    def gate_block(c, k):
+        x = arr[c]
+        g, u = (
+            lax.dot_general(
                 x,
-                wg[k * zh : (k + 1) * zh].reshape(hw, width),
+                w[k * zh : (k + 1) * zh].reshape(hw, width),
                 dims,
                 preferred_element_type=F32,
             )
-            u = lax.dot_general(
-                x,
-                wu[k * zh : (k + 1) * zh].reshape(hw, width),
-                dims,
-                preferred_element_type=F32,
-            )
-            hid[core, pl.ds(hint(n * hm, hm), hm), k * hw : (k + 1) * hw] = (
-                g * jax.nn.sigmoid(g) * u
-            ).astype(BF16)
-        return 0
-
-    lax.fori_loop(0, 2 * per, gate_body, 0)
-    swap = pltpu.make_async_remote_copy(
-        src_ref=hid.at[core],
-        dst_ref=hid.at[core],
-        send_sem=hid_sem.at[0],
-        recv_sem=hid_sem.at[1],
-        device_id=(sp, sibling),
-        device_id_type=MESH,
-    )
-    swap.start()
-    advance(1)
-    swap.wait_recv()
+            for w in (wg, wu)
+        )
+        hid[core, pl.ds(hint(c * slots, slots), slots), k * hw : (k + 1) * hw] = (
+            g * jax.nn.sigmoid(g) * u
+        ).astype(BF16)
+        swap(c, k).start()
+        drains.append(swap(c, k).wait_send)
+        poll()
+
+    need(l_wg)
+    need(l_wu)
+    blocks = hidden_all // hw
+    for k in range(blocks):
+        last = k == blocks - 1
+        if last:
+            poll()
+        complete(0, zh * (k + 1))
+        complete(1, zh * (k + 1))
+        if last:
+            poll()
+        gate_block(core, k)
+        if k == 0:
+            blocked_all(arr.at[other], fwd_sem.at[1])
+        gate_block(other, k)
+    poll()
+    for k in range(blocks):
+        for c in range(2):
+            swap(c, k).wait_recv()
 
     for q in range(CHUNKS):
-        while not all(
-            any(ev == (p, h) for ev in plans[d][: place[d]])
-            for d in (0, 1)
-            for p, h in plans[d]
-            if p == 2 + q
-        ):
-            advance(1)
-        advance(1)
+        cols = slice(STARTS[q], STARTS[q] + WIDTHS[q])
+        poll()
+        poll()
         complete(2 + q)
+        poll()
+
+        hm = min(256, slots)
 
         def down_body(n, _):
             at = pl.ds(hint(n * hm, hm), hm)
             o = jnp.dot(
-                hid[0, at, :], wd[0, :, q * cw : (q + 1) * cw], preferred_element_type=F32
-            ) + jnp.dot(hid[1, at, :], wd[1, :, q * cw : (q + 1) * cw], preferred_element_type=F32)
-            outb[q, at, :] = o.astype(BF16)
+                hid[0, at, :], wd[0, :, cols], preferred_element_type=F32
+            ) + jnp.dot(hid[1, at, :], wd[1, :, cols], preferred_element_type=F32)
+            outb[q][at, :] = o.astype(BF16)
             return 0
 
-        lax.fori_loop(0, 2 * per, down_body, 0)
+        lax.fori_loop(0, 2 * slots // hm, down_body, 0)
+        poll()
         for i in range(n_sp):
             peer = lax.rem(sp + i, n_sp)
             for mine in (1, 0):
@@ -599,26 +701,32 @@
                     continue
                 c = core if mine else other
                 pltpu.make_async_remote_copy(
-                    src_ref=outb.at[q, pl.ds(hint(c * slots + peer * cap, cap), cap), :],
-                    dst_ref=ret.at[core, q, own_slots, :],
+                    src_ref=outb[q].at[pl.ds(hint(c * slots + peer * cap, cap), cap), :],
+                    dst_ref=ret[q].at[core, own_slots, :],
                     send_sem=ret_send.at[q, mine],
                     recv_sem=ret_recv.at[q, mine],
                     device_id=(peer, tp if mine else sibling),
                     device_id_type=MESH,
                 ).start()
-        ret[core, q, own_slots, :] = outb[
-            q, pl.ds(hint(core * slots + sp * cap, cap), cap), :
+        drains.append(
+            lambda q=q: blocked_all(ret[q].at[core, 0 : slots - cap, :], ret_send.at[q, 1])
+        )
+        drains.append(lambda q=q: blocked_all(ret[q].at[other], ret_send.at[q, 0]))
+        ret[q][core, own_slots, :] = outb[q][
+            pl.ds(hint(core * slots + sp * cap, cap), cap), :
         ]
+        poll()
 
     for q in range(CHUNKS):
-        blocked_all(ret.at[core, q, 0 : slots - cap, :], ret_recv.at[q, 1])
-        blocked_all(ret.at[other, q], ret_recv.at[q, 0])
+        blocked_all(ret[q].at[core, 0 : slots - cap, :], ret_recv.at[q, 1])
+        blocked_all(ret[q].at[other], ret_recv.at[q, 0])
         for c in range(2):
-            v = ret[c, q]
+            v = ret[q][c]
             o = jnp.dot(wtab[0], v, preferred_element_type=F32) + jnp.dot(
                 wtab[1], v, preferred_element_type=F32
             )
-            pbuf[:, c * half + q * cw : c * half + (q + 1) * cw] = o.astype(BF16).astype(F32)
+            at = c * half + STARTS[q]
+            pbuf[:, at : at + WIDTHS[q]] = o.astype(BF16).astype(F32)
 
     def final_body(n, _):
         at = pl.ds(hint(n * 16, 16), 16)
@@ -628,16 +736,7 @@
 
     lax.fori_loop(0, rows // 16, final_body, 0)
 
-    blocked_all(stats.at[0 : n_sp - 1], stat_sem.at[0])
-    blocked_all(tokb.at[:, 0 : (n_tp - 1) * chans], tok_sem.at[0])
-    blocked_all(outg.at[0 : slots - cap, :], disp_send.at[0])
-    blocked_all(outg, fwd_sem.at[0])
-    swap.wait_send()
-    for q in range(CHUNKS):
-        blocked_all(ret.at[core, q, 0 : slots - cap, :], ret_send.at[q, 1])
-        blocked_all(ret.at[other, q], ret_send.at[q, 0])
-    for event in sent:
-        ring_copy(*event).wait_send()
+    finish()
 
 
 def on_device(
@@ -672,10 +771,7 @@
     far = nz // 2
     pieces = 2 + CHUNKS
 
-    def tables(array):
-        return array.T.reshape(top, n_tp, rows).transpose(1, 0, 2)
-
-    anywhere = pl.BlockSpec(memory_space=pl.ANY)
+    anywhere = pl.BlockSpec(memory_space=pltpu.HBM)
     onchip = pl.BlockSpec(memory_space=pltpu.VMEM)
     dma = pltpu.SemaphoreType.DMA
     scratch = [
@@ -683,8 +779,8 @@
         pltpu.VMEM((seq, chans), BF16),
         pltpu.VMEM((rows, width), BF16),
         pltpu.VMEM(out_proj.shape, BF16),
-        pltpu.VMEM((n_tp, top, rows), jnp.int32),
-        pltpu.VMEM((n_tp, top, rows), F32),
+        pltpu.VMEM((top, 2 * rows), jnp.int32),
+        pltpu.VMEM((top, 2 * rows), F32),
         pltpu.VMEM((2, 16, chans), BF16),
         pltpu.VMEM((seq + 16, chans), F32),
         pltpu.VMEM((seq, chans), F32),
@@ -705,8 +801,8 @@
         pltpu.VMEM((nz, hs, width), BF16),
         pltpu.VMEM((2, nz * hs, half), BF16),
         pltpu.VMEM((2, 2 * slots, nz * hs), BF16),
-        pltpu.VMEM((CHUNKS, 2 * slots, half // CHUNKS), BF16),
-        pltpu.VMEM((2, CHUNKS, slots, half // CHUNKS), BF16),
+        [pltpu.VMEM((2 * slots, w), BF16) for w in WIDTHS],
+        [pltpu.VMEM((2, slots, w), BF16) for w in WIDTHS],
         pltpu.VMEM((2, rows, slots), BF16),
         dma((9,)),
         dma((2,)),
@@ -716,7 +812,8 @@
         dma((1,)),
         dma((n_sp - 1,)),
         dma((2,)),
-        dma((2,)),
+        dma((2, nz * hs // min(256, nz * hs))),
+        dma((2, nz * hs // min(256, nz * hs))),
         dma((2,)),
         dma((2, pieces, far)),
         dma((2, pieces, far)),
@@ -764,8 +861,8 @@
         residual,
         out_proj,
         norm_gain,
-        tables(routes),
-        tables(route_wt),
+        routes.T,
+        route_wt.T,
         exp_gate[0].T,
         exp_up[0].T,
         exp_down[0],

time: 107 us -> 94.3 us (0.88)
  Pallas kernels: 103 us -> 92.5 us
  local copies, waits for them, and re-layouts: 4.45 us -> 1.67 us
    pallas_call x1, Pallas kernels: 103 us -> 92.5 us  [on_device(): pl.pallas_call(functools.partial(kernel, n_sp, n_tp), out_shape=jax.Shape...]
    reshape x4 -> x0, local copies, waits for them, and re-layouts: 2.78 us -> none  [tables(): return array.T.reshape(top, n_tp, rows).transpose(1, 0, 2)]
where the time goes in v2:
time: 94.3 us; the launch traced here: 94.2 us
  Pallas kernels  92.5 us (98%)
  local copies, waits for them, and re-layouts  1.67 us (2%)
    pallas_call x1, Pallas kernels, on_device(): pl.pallas_call(functools.partial(kernel, n_sp, n_tp), out_shape=jax.Shape...  92.5 us

profile of v2, /device:TPU:1, one launch (start us, length us, event | category | flops | bytes accessed | tf_op | source)
XLA Modules:
  0.0 94.2 jit_solution(18101130975713652795)
XLA Ops:
  0.0 92.5 %shard_map.163 = bf16[64,2048]{1,0:T(8,128)(2,1)} custom-call(bf16[1024,128]{1,0:T(8,128)(2,1)} %mix_h.1, bf16[1024,128]{1,0:T(8,128)(2,1)} %gate_h.1, f32[4,128]{1,0:T(4,128)} %conv_w.1, f32[1,128]{1,0:T(1,128)} %bitcast.15, f32[2,128]{1,0:T(2,128)} %decay.1, f32[2,2,64,64]{3,2,1,0:T(8,128)} %rg.1, f32[2,128]{1,0:T(2,128)} %rb.1, f32[2,2,64,64]{3,2,1,0:T(8,128)} %ig.1, ...), custom_call_target="tpu_custom_call" | custom-call | tf_op jit(solution)/shard_map/pallas_call | solution.py:842
  92.5 1.7 %copy.19 = bf16[64,2048]{1,0:T(8,128)(2,1)} copy(bf16[64,2048]{1,0:T(8,128)(2,1)} %shard_map.163) | data formatting | bytes 524288

commit v3 on v2

--- a/solution.py
+++ b/solution.py
@@ -155,6 +155,7 @@
     outb,
     ret,
     wtab,
+    known,
     load_sem,
     halo_send,
     halo_recv,
@@ -214,12 +215,13 @@
     l_wt = load(wts_h.at[:, pair], wtsv, 8)
 
     barrier = pltpu.get_barrier_semaphore()
-    partners = []
-    for i in range(1, n_sp):
-        peer = lax.rem(sp + i, n_sp)
-        partners += [(peer, tp), (peer, sibling)]
-    for i in range(1, n_tp):
-        partners.append((sp, lax.rem(tp + i, n_tp)))
+    side = 4
+    x, y = lax.rem(sp, side), sp // side
+    near_by = [(sp, sibling)]
+    near_by += [(sp, lax.rem(tp + n_tp + 2 * step, n_tp)) for step in (1, -1)]
+    near_by += [(y * side + lax.rem(x + side + step, side), tp) for step in (1, -1)]
+    near_by += [(lax.rem(sp + n_sp + side * step, n_sp), tp) for step in (1, -1)]
+    partners = near_by + [(lax.rem(sp + n_sp + step, n_sp), tp) for step in (1, -1)]
     for peer in partners:
         pl.semaphore_signal(barrier, inc=1, device_id=peer, device_id_type=MESH)
 
@@ -232,7 +234,38 @@
                 wcat[h * hd : (h + 1) * hd, at : at + hd] = ref[d, h]
 
     need(l_mix)
+
+    xpad[0:8, :] = jnp.zeros((8, chans), F32)
+    xpad[8 : 8 + seq, :] = mixv[...].astype(F32)
+    xpad[8 + seq : 16 + seq, :] = jnp.zeros((8, chans), F32)
+
+    def strided(t):
+        return xpad[pl.ds(t, SEGMENTS, stride=seg), :]
+
+    taps = [jnp.broadcast_to(conv_w[j : j + 1, :], (SEGMENTS, chans)) for j in range(4)]
+    bias = jnp.broadcast_to(conv_b[0:1, :], (SEGMENTS, chans))
+
+    def weigh(x0, x1, x2, x3):
+        return bias + x0 * taps[0] + x1 * taps[1] + x2 * taps[2] + x3 * taps[3]
+
+    def conv_body(t, window):
+        x0, x1, x2 = window
+        x3 = strided(9 + t)
+        conv_s[pl.ds(hint(t * SEGMENTS, SEGMENTS), SEGMENTS), :] = weigh(x0, x1, x2, x3)
+        return x1, x2, x3
+
+    lax.fori_loop(0, seg, conv_body, (strided(6), strided(7), strided(8)), unroll=8)
+
     pl.semaphore_wait(barrier, len(partners))
+
+    def tell(k):
+        for peer in near_by:
+            pl.semaphore_signal(known.at[k], inc=1, device_id=peer, device_id_type=MESH)
+
+    def hear(k):
+        pl.semaphore_wait(known.at[k], len(near_by))
+
+    tell(0)
 
     right = 2 * lax.rem(z + 1, nz) + core
     left = 2 * lax.rem(z + nz - 1, nz) + core
@@ -330,27 +363,6 @@
     )
     poll()
     pre.start()
-
-    xpad[0:8, :] = jnp.zeros((8, chans), F32)
-    xpad[8 : 8 + seq, :] = mixv[...].astype(F32)
-    xpad[8 + seq : 16 + seq, :] = jnp.zeros((8, chans), F32)
-
-    def strided(t):
-        return xpad[pl.ds(t, SEGMENTS, stride=seg), :]
-
-    taps = [jnp.broadcast_to(conv_w[j : j + 1, :], (SEGMENTS, chans)) for j in range(4)]
-    bias = jnp.broadcast_to(conv_b[0:1, :], (SEGMENTS, chans))
-
-    def weigh(x0, x1, x2, x3):
-        return bias + x0 * taps[0] + x1 * taps[1] + x2 * taps[2] + x3 * taps[3]
-
-    def conv_body(t, window):
-        x0, x1, x2 = window
-        x3 = strided(9 + t)
-        conv_s[pl.ds(hint(t * SEGMENTS, SEGMENTS), SEGMENTS), :] = weigh(x0, x1, x2, x3)
-        return x1, x2, x3
-
-    lax.fori_loop(0, seg, conv_body, (strided(6), strided(7), strided(8)), unroll=8)
 
     rates = []
     for d in range(2):
@@ -385,8 +397,12 @@
         return 0
 
     lax.fori_loop(0, seq // part // 2, coef_body, 0)
+    hear(0)
+    tell(1)
     poll()
     lax.fori_loop(seq // part // 2, seq // part, coef_body, 0)
+    hear(1)
+    tell(2)
 
     poll()
     to_next.wait()
@@ -423,6 +439,8 @@
     f_end, p_end, g_end, q_end = lax.fori_loop(0, seg, scan_body, (zero, one, zero, one), unroll=8)
 
     poll()
+    hear(2)
+    tell(3)
 
     row = lambda v, k: v[k : k + 1, :]
     f_scale, f_shift = [row(one, 0)], [row(zero, 0)]
@@ -489,6 +507,7 @@
     lax.fori_loop(0, seq // rows, mix_body, 0)
     poll()
 
+    hear(3)
     own_cols = pl.ds(hint(tp * chans, chans), chans)
     for i in range(1, n_tp):
         peer = lax.rem(tp + i, n_tp)
@@ -804,6 +823,7 @@
         [pltpu.VMEM((2 * slots, w), BF16) for w in WIDTHS],
         [pltpu.VMEM((2, slots, w), BF16) for w in WIDTHS],
         pltpu.VMEM((2, rows, slots), BF16),
+        pltpu.SemaphoreType.REGULAR((4,)),
         dma((9,)),
         dma((2,)),
         dma((2,)),

time: 94.3 us -> 92.7 us (0.983)
  Pallas kernels: 92.5 us -> 90.9 us
    pallas_call x1, Pallas kernels: 92.5 us -> 90.9 us  [on_device(): pl.pallas_call(functools.partial(kernel, n_sp, n_tp), out_shape=jax.Shape...]
where the time goes in v3:
time: 92.7 us; the launch traced here: 92.6 us
  Pallas kernels  90.9 us (98%)
  local copies, waits for them, and re-layouts  1.67 us (2%)
    pallas_call x1, Pallas kernels, on_device(): pl.pallas_call(functools.partial(kernel, n_sp, n_tp), out_shape=jax.Shape...  90.9 us

profile of v3, /device:TPU:1, one launch (start us, length us, event | category | flops | bytes accessed | tf_op | source)
XLA Modules:
  0.0 92.6 jit_solution(6977293386728058137)
XLA Ops:
  0.0 90.9 %shard_map.163 = bf16[64,2048]{1,0:T(8,128)(2,1)} custom-call(bf16[1024,128]{1,0:T(8,128)(2,1)} %mix_h.1, bf16[1024,128]{1,0:T(8,128)(2,1)} %gate_h.1, f32[4,128]{1,0:T(4,128)} %conv_w.1, f32[1,128]{1,0:T(1,128)} %bitcast.15, f32[2,128]{1,0:T(2,128)} %decay.1, f32[2,2,64,64]{3,2,1,0:T(8,128)} %rg.1, f32[2,128]{1,0:T(2,128)} %rb.1, f32[2,2,64,64]{3,2,1,0:T(8,128)} %ig.1, ...), custom_call_target="tpu_custom_call" | custom-call | tf_op jit(solution)/shard_map/pallas_call | solution.py:862
  90.9 1.7 %copy.19 = bf16[64,2048]{1,0:T(8,128)(2,1)} copy(bf16[64,2048]{1,0:T(8,128)(2,1)} %shard_map.163) | data formatting | bytes 524288

commit v4 on v3

--- a/solution.py
+++ b/solution.py
@@ -18,58 +18,58 @@
 PLAN = (
     ((0, 0, 1), (0, 1, 1), (1, 1, 1), (1, 0, 1),),
     (),
-    ((0, 4, 1), (0, 5, 1), (0, 2, 1), (0, 3, 1), (1, 4, 1), (1, 5, 1), (1, 2, 1), (1, 3, 1),),
+    ((0, 2, 1), (0, 3, 1), (0, 4, 1), (0, 5, 1), (1, 2, 1), (1, 3, 1), (1, 4, 1), (1, 5, 1),),
     (),
     (),
     (),
     ((0, 0, 2), (1, 1, 2),),
     (),
-    ((0, 1, 2), (1, 0, 2), (0, 0, 3), (1, 2, 2), (1, 1, 3),),
-    (),
-    (),
-    (),
-    (),
-    (),
-    ((0, 2, 2), (0, 3, 2), (0, 4, 2), (0, 5, 2), (0, 6, 1), (1, 3, 2), (1, 4, 2), (1, 5, 2), (1, 6, 1), (0, 1, 3), (1, 7, 1), (1, 2, 3),),
-    (),
-    ((1, 0, 3),),
-    (),
+    ((0, 1, 2), (1, 0, 2), (0, 4, 2), (0, 5, 2), (0, 2, 2), (0, 3, 2), (0, 0, 3), (1, 4, 2), (1, 5, 2), (1, 2, 2), (1, 3, 2), (1, 1, 3),),
+    (),
+    (),
+    (),
+    (),
+    (),
+    ((0, 6, 1), (1, 6, 1), (0, 1, 3), (1, 7, 1), (1, 0, 3),),
     (),
     (),
     (),
     ((0, 2, 3),),
-    ((0, 3, 3), (1, 3, 3),),
-    (),
+    ((0, 3, 3),),
+    ((1, 2, 3),),
+    ((1, 3, 3),),
     (),
     ((0, 0, 4), (1, 1, 4),),
     (),
     (),
     (),
     (),
-    ((0, 6, 2), (0, 7, 1), (0, 4, 3), (1, 6, 2), (1, 7, 2),),
-    (),
-    ((0, 2, 4), (1, 3, 4),),
-    ((0, 6, 3), (1, 4, 3),),
-    ((1, 5, 3),),
-    ((0, 4, 4), (1, 6, 3),),
-    ((0, 7, 2),),
-    (),
+    (),
+    (),
+    ((0, 6, 2), (0, 7, 1), (0, 4, 3), (0, 5, 3), (1, 6, 2), (1, 7, 2), (1, 4, 3),),
+    (),
+    ((0, 2, 4), (1, 5, 3), (1, 3, 4),),
+    ((0, 6, 3),),
+    (),
+    ((0, 7, 2), (1, 6, 3), (0, 4, 4),),
     (),
     (),
     ((1, 7, 3),),
     (),
-    (),
-    (),
-    ((0, 5, 3),),
-    (),
-    (),
-    (),
-    ((0, 6, 4), (1, 5, 4),),
-    (),
-    (),
-    (),
-    (),
-    ((0, 7, 3), (1, 7, 4),),
+    ((1, 5, 4),),
+    (),
+    (),
+    (),
+    (),
+    ((0, 6, 4),),
+    (),
+    (),
+    ((0, 7, 3),),
+    (),
+    (),
+    (),
+    (),
+    ((1, 7, 4),),
     (),
     (),
     (),

time: 92.7 us -> 92 us (level)
  no operation moved by 1% of the time
where the time goes in v4:
time: 92 us; the launch traced here: 91.8 us
  Pallas kernels  90.2 us (98%)
  local copies, waits for them, and re-layouts  1.67 us (2%)
    pallas_call x1, Pallas kernels, on_device(): pl.pallas_call(functools.partial(kernel, n_sp, n_tp), out_shape=jax.Shape...  90.2 us

profile of v4, /device:TPU:1, one launch (start us, length us, event | category | flops | bytes accessed | tf_op | source)
XLA Modules:
  0.0 91.8 jit_solution(16925150049272612173)
XLA Ops:
  0.0 90.2 %shard_map.163 = bf16[64,2048]{1,0:T(8,128)(2,1)} custom-call(bf16[1024,128]{1,0:T(8,128)(2,1)} %mix_h.1, bf16[1024,128]{1,0:T(8,128)(2,1)} %gate_h.1, f32[4,128]{1,0:T(4,128)} %conv_w.1, f32[1,128]{1,0:T(1,128)} %bitcast.15, f32[2,128]{1,0:T(2,128)} %decay.1, f32[2,2,64,64]{3,2,1,0:T(8,128)} %rg.1, f32[2,128]{1,0:T(2,128)} %rb.1, f32[2,2,64,64]{3,2,1,0:T(8,128)} %ig.1, ...), custom_call_target="tpu_custom_call" | custom-call | tf_op jit(solution)/shard_map/pallas_call | solution.py:862
  90.2 1.7 %copy.19 = bf16[64,2048]{1,0:T(8,128)(2,1)} copy(bf16[64,2048]{1,0:T(8,128)(2,1)} %shard_map.163) | data formatting | bytes 524288

commit v5 on v4

--- a/solution.py
+++ b/solution.py
@@ -565,8 +565,8 @@
         preferred_element_type=F32,
     )
     high = table.astype(BF16)
-    wtab[0] = high
-    wtab[1] = (table - high.astype(F32)).astype(BF16)
+    wtab[0:rows, :] = high
+    wtab[rows : 2 * rows, :] = (table - high.astype(F32)).astype(BF16)
 
     need(l_op)
     need(l_res)
@@ -741,9 +741,8 @@
         blocked_all(ret[q].at[other], ret_recv.at[q, 0])
         for c in range(2):
             v = ret[q][c]
-            o = jnp.dot(wtab[0], v, preferred_element_type=F32) + jnp.dot(
-                wtab[1], v, preferred_element_type=F32
-            )
+            both = jnp.dot(wtab[...], v, preferred_element_type=F32)
+            o = both[0:rows] + both[rows : 2 * rows]
             at = c * half + STARTS[q]
             pbuf[:, at : at + WIDTHS[q]] = o.astype(BF16).astype(F32)
 
@@ -822,7 +821,7 @@
         pltpu.VMEM((2, 2 * slots, nz * hs), BF16),
         [pltpu.VMEM((2 * slots, w), BF16) for w in WIDTHS],
         [pltpu.VMEM((2, slots, w), BF16) for w in WIDTHS],
-        pltpu.VMEM((2, rows, slots), BF16),
+        pltpu.VMEM((2 * rows, slots), BF16),
         pltpu.SemaphoreType.REGULAR((4,)),
         dma((9,)),
         dma((2,)),

time: 92 us -> 91.9 us (level)
  no operation moved by 1% of the time
where the time goes in v5:
time: 91.9 us; the launch traced here: 91.8 us
  Pallas kernels  90.1 us (98%)
  local copies, waits for them, and re-layouts  1.67 us (2%)
    pallas_call x1, Pallas kernels, on_device(): pl.pallas_call(functools.partial(kernel, n_sp, n_tp), out_shape=jax.Shape...  90.1 us

profile of v5, /device:TPU:1, one launch (start us, length us, event | category | flops | bytes accessed | tf_op | source)
XLA Modules:
  0.0 91.8 jit_solution(4291394191408375325)
XLA Ops:
  0.0 90.1 %shard_map.163 = bf16[64,2048]{1,0:T(8,128)(2,1)} custom-call(bf16[1024,128]{1,0:T(8,128)(2,1)} %mix_h.1, bf16[1024,128]{1,0:T(8,128)(2,1)} %gate_h.1, f32[4,128]{1,0:T(4,128)} %conv_w.1, f32[1,128]{1,0:T(1,128)} %bitcast.15, f32[2,128]{1,0:T(2,128)} %decay.1, f32[2,2,64,64]{3,2,1,0:T(8,128)} %rg.1, f32[2,128]{1,0:T(2,128)} %rb.1, f32[2,2,64,64]{3,2,1,0:T(8,128)} %ig.1, ...), custom_call_target="tpu_custom_call" | custom-call | tf_op jit(solution)/shard_map/pallas_call | solution.py:861
  90.2 1.7 %copy.19 = bf16[64,2048]{1,0:T(8,128)(2,1)} copy(bf16[64,2048]{1,0:T(8,128)(2,1)} %shard_map.163) | data formatting | bytes 524288
